TPU v7x, 512 devices: a whole 4x4x16 slice. The times are simulated.
512 devices in a mesh: sp: 32 (over z, core), tp: 16 (over y, x).
Axes of the slice: x: 4, y: 4, z: 16, core: 2. Of those that a mesh axis runs over, the one named last changes fastest.
Arguments:
- out_gate: bfloat16 [8192, 512], P('sp', 'tp'), may hold values from -6 to 6
- in_gate: bfloat16 [8192, 512], P('sp', 'tp'), may hold values from -6 to 6
- conv_input: bfloat16 [8192, 512], P('sp', 'tp'), may hold values from -6 to 6
- conv_taps: float32 [3, 512], P(None, 'tp'), may hold values from -3.5 to 3.5
- out_weight: bfloat16 [512, 2048], P('tp'), may hold values from -0.25 to 0.25
- residual: bfloat16 [8192, 2048], P('sp', 'tp'), may hold values from -60 to 60
- document: int32 [8192], P('sp'), may hold values from 0 to 7, never falling along the last dimension, each value on 1 to 2048 neighbouring positions
- mix_gain: float32 [2048], P('tp'), may hold values from 0.15 to 3
- ffn_gain: float32 [2048], P('tp'), may hold values from 0.1 to 1.9
- routes: int32 [8192, 2], P('sp'), may hold values from 0 to 31, all different within a row; in each aligned block of 256 rows (0 to 255, 256 to 511, ...) at most 32 rows name the same one
- route_weight: float32 [8192, 2], P('sp'), may hold values from 0.1 to 1
- expert_gate: bfloat16 [32, 2048, 4096], P('sp', None, 'tp'), may hold values from -0.375 to 0.375
- expert_up: bfloat16 [32, 2048, 4096], P('sp', None, 'tp'), may hold values from -0.375 to 0.375
- expert_down: bfloat16 [32, 4096, 2048], P('sp', None, 'tp'), may hold values from -0.09375 to 0.09375
Outputs:
- result: bfloat16 [8192, 2048], P('sp', 'tp')
Inputs may be any that keep to these rules, and one draw needn't show every extreme that they name: `routes`: within each aligned block of 256 rows, no expert is named more than 32 times; some expert is named exactly 32 times in some blocks. The 2 experts of a row differ. Document numbers never fall along the positions; each document is one contiguous run.
All inputs are finite; a program needn't handle non-finite values.
Results may differ from a plain program's by a relative error of at most 0.0069.
Values may be sent and summed in bfloat16 or wider, within the bound.
A program may use at most 64 MiB of HBM per device.

v0:
```python
import functools

import jax
import jax.numpy as jnp
from jax import lax
from jax.sharding import Mesh
from jax.sharding import PartitionSpec as P

D = 2048
TP = ("tp_0", "tp_1")


ALPHA = 8.0**0.25
EPSILON = 1e-05
LIMIT = 7.0
SLOPE = 1.702


def over_axes(value, axes):
    return functools.reduce(lax.psum, axes, value)


def from_behind(value, axis, steps):
    count = lax.axis_size(axis)
    initial, last = (max(0, -steps), min(count, count - steps))
    return lax.ppermute(value, axis, [(source, source + steps) for source in range(initial, last)])


def joined_along(tiles, dim):
    lengths = list(tiles.shape[1:])
    lengths[dim] *= tiles.shape[0]
    return jnp.moveaxis(tiles, 0, dim).reshape(lengths)


def copy_for_each(value, axis):
    devices = lax.axis_size(axis)
    return lax.all_to_all(
        jnp.broadcast_to(value[None], (devices, *value.shape)), axis, 0, 0, tiled=True
    )


def gathered_copies(value, axis, dim):
    return joined_along(copy_for_each(value, axis), dim)


def split_norm(stream, gain_row):
    row_sums = jnp.sum(stream, axis=1)
    row_squares = jnp.sum(stream * stream, axis=1)
    row_sums, row_squares = (over_axes(row_sums, TP), over_axes(row_squares, TP))
    row_mean = row_sums / D
    row_spread = row_squares / D - row_mean * row_mean
    scaled = (stream - row_mean[:, None]) * lax.rsqrt(row_spread + EPSILON)[:, None]
    return (scaled * gain_row[None, :]).astype(jnp.bfloat16)


def clamped_unit(gate_pre, up_pre):
    gate_part = jnp.minimum(gate_pre, LIMIT)
    up_part = jnp.clip(up_pre, -LIMIT, LIMIT)
    return ((up_part + 1.0) * gate_part * jax.nn.sigmoid(SLOPE * gate_part)).astype(jnp.bfloat16)


def project_down(hidden, weight_down):
    summed = jnp.dot(
        lax.all_gather(hidden, TP, axis=1, tiled=True),
        weight_down,
        preferred_element_type=jnp.float32,
    )
    return summed.astype(jnp.bfloat16)


def per_device(
    out_gate,
    in_gate,
    conv_input,
    conv_taps,
    out_weight,
    residual,
    document,
    mix_gain,
    ffn_gain,
    routes,
    route_weight,
    expert_gate,
    expert_up,
    expert_down,
):
    product = in_gate.astype(jnp.float32) * conv_input.astype(jnp.float32)
    doc_marks = document.astype(jnp.float32)
    prior_rows, prior_marks = from_behind((product[-2:], doc_marks[-2:]), "sp", 1)
    row_count = product.shape[0]
    extended = jnp.concatenate([prior_rows, product], axis=0)
    extended_marks = jnp.concatenate([prior_marks, doc_marks], axis=0)
    same_one = (extended_marks[1 : row_count + 1] == doc_marks).astype(jnp.float32)[:, None]
    same_two = (extended_marks[0:row_count] == doc_marks).astype(jnp.float32)[:, None]
    mixed_rows = (
        conv_taps[2][None, :] * product
        + same_one * conv_taps[1][None, :] * extended[1 : row_count + 1]
        + same_two * conv_taps[0][None, :] * extended[0:row_count]
    )
    conv_out = (out_gate.astype(jnp.float32) * mixed_rows).astype(jnp.bfloat16)
    weight_cols = lax.all_to_all(out_weight, TP, split_axis=1, concat_axis=0, tiled=True)
    mixer_sum = jnp.dot(
        gathered_copies(conv_out, TP, 1), weight_cols, preferred_element_type=jnp.float32
    )
    normed = split_norm(ALPHA * residual.astype(jnp.float32) + mixer_sum, mix_gain)
    expert_count = lax.axis_size("sp")
    token_count = routes.shape[0]
    top_count = routes.shape[1]
    capacity = 2 * token_count * top_count // expert_count
    flat_routes = routes.reshape(-1)
    one_hot = (flat_routes[:, None] == jnp.arange(expert_count, dtype=jnp.int32)[None, :]).astype(
        jnp.int32
    )
    rank_table = jnp.cumsum(one_hot, axis=0) - one_hot
    slot_index = jnp.sum(rank_table * one_hot, axis=1)
    target_slot = flat_routes * capacity + slot_index
    source_rows = jnp.arange(token_count * top_count, dtype=jnp.int32) // top_count
    weight_gate = expert_gate[0]
    weight_up = expert_up[0]
    weight_down = expert_down[0]
    send_buffer = (
        jnp.zeros((expert_count * capacity, normed.shape[1]), jnp.bfloat16)
        .at[target_slot]
        .set(normed[source_rows])
    )
    received = lax.all_to_all(
        send_buffer.reshape(expert_count, capacity, normed.shape[1]),
        "sp",
        split_axis=0,
        concat_axis=0,
        tiled=True,
    )
    flat_rows = received.reshape(-1, received.shape[2])
    shard_piece = lax.all_gather(flat_rows, TP, axis=1, tiled=True)
    gate_pre = jnp.dot(shard_piece, weight_gate, preferred_element_type=jnp.float32)
    up_pre = jnp.dot(shard_piece, weight_up, preferred_element_type=jnp.float32)
    expert_out = project_down(clamped_unit(gate_pre, up_pre), weight_down)
    computed = expert_out.reshape(received.shape[0], received.shape[1], expert_out.shape[1])
    returned = lax.all_to_all(computed, "sp", split_axis=0, concat_axis=0, tiled=True).reshape(
        expert_count * capacity, -1
    )
    picked = returned[target_slot].astype(jnp.float32).reshape(token_count, top_count, -1)
    ffn_out = jnp.sum(picked * route_weight[:, :, None], axis=1)
    return split_norm(ALPHA * normed.astype(jnp.float32) + ffn_out, ffn_gain)


def solution(mesh):
    torus = Mesh(mesh.devices.reshape(mesh.shape["sp"], 4, 4), ("sp", "tp_0", "tp_1"))
    in_specs = (
        P("sp", TP),
        P("sp", TP),
        P("sp", TP),
        P(None, TP),
        P(TP, None),
        P("sp", TP),
        P("sp"),
        P(TP),
        P(TP),
        P("sp", None),
        P("sp", None),
        P("sp", None, TP),
        P("sp", None, TP),
        P("sp", None, TP),
    )
    out_specs = P("sp", TP)
    return jax.shard_map(
        per_device, mesh=torus, in_specs=in_specs, out_specs=out_specs, check_vma=False
    )
```

profile of v0, /device:TPU:1, one launch (start us, length us, event | category | flops | bytes accessed | tf_op | source)
XLA Modules:
  0.0 328.3 jit_solution(5198498614145085097)
XLA Ops:
  6.5 0.0 copy-start
  6.5 0.8 convert_element_type.57
  7.3 0.1 slice.34
  7.4 4.9 %collective-permute-start = (f32[2]{0:T(128)S(1)}, f32[2]{0:T(128)S(1)}, u32[]{:S(2)}, u32[]{:S(2)}) collective-permute-start(f32[2]{0:T(128)S(1)} %slice.34), channel_id=1, source_target_pairs={{0,16},{16,32},{32,48},{48,64},{64,80},{80,96},{96,112},{112,128},... | collective-permute-start | bytes 32 | tf_op jit(solution)/shard_map/ppermute | solution.py:26
  12.3 0.7 convert_multiply_fusion.1
  13.0 0.1 slice.48
  13.1 1.9 collective-permute-start.1
  15.0 1.6 copy_bitcast_fusion
  16.6 6.8 %all-to-all-start.1 = ((bf16[32,16,128]{2,0,1:T(8,128)(2,1)}), bf16[32,16,128]{2,0,1:T(8,128)(2,1)S(1)}, u32[]{:S(2)}, u32[]{:S(2)}) async-start(bf16[32,16,128]{2,0,1:T(8,128)(2,1)} %copy_bitcast_fusion), calls=%async_computation.1 | async-start | bytes 262144 | tf_op jit(solution)/shard_map/all_to_all | solution.py:101
  23.4 0.8 copy.31
  24.2 0.1 eq.37
  24.3 0.1 eq.33
  24.5 0.7 broadcast_multiply_fusion
  25.2 0.8 slice_bitcast_fusion.2
  26.0 1.2 reduce-window.6
  27.2 0.2 slice_reduce_fusion
  27.4 0.1 fusion.16
  27.5 0.0 collective-permute-done
  27.5 0.1 pad_maximum_fusion.1
  27.6 0.8 compare_convert_fusion.1
  28.4 0.0 collective-permute-done.1
  28.4 0.8 fusion.24
  29.2 1.0 all-to-all-done.1
  30.2 0.7 broadcast_in_dim.4
  30.9 5.7 %all-to-all-start = ((bf16[16,256,32]{1,2,0:T(8,128)(2,1)}), bf16[16,256,32]{1,2,0:T(8,128)(2,1)S(1)}, u32[]{:S(2)}, u32[]{:S(2)}) async-start(bf16[16,256,32]{1,2,0:T(8,128)(2,1)} %broadcast_in_dim.4), calls=%async_computation | async-start | bytes 524288 | tf_op jit(solution)/shard_map/all_to_all | solution.py:37
  36.6 0.0 all-gather.3.cloned.1.call-start
  36.6 0.9 copy.28
  37.6 0.1 copy.30
  37.7 0.1 mul.166
  37.9 6.3 %all-to-all-done = bf16[16,256,32]{1,2,0:T(8,128)(2,1)S(1)} async-done(((bf16[16,256,32]{1,2,0:T(8,128)(2,1)}), bf16[16,256,32]{1,2,0:T(8,128)(2,1)S(1)}, u32[]{:S(2)}, u32[]{:S(2)}) %all-to-all-start) | async-done | bytes 262176 | tf_op jit(solution)/shard_map/all_to_all | solution.py:37
  44.2 0.2 fusion.26
  44.5 6.7 %all-reduce.3 = (f32[256]{0:T(256)S(1)}, f32[256]{0:T(256)S(1)}) all-reduce(f32[256]{0:T(256)S(1)} %get-tuple-element.8, f32[256]{0:T(256)S(1)} %get-tuple-element.7), channel_id=1, replica_groups=mesh['sp'=32,'tp_0'=4,'tp_1'=4] {'tp_0'}, use_global_device_ids=true, to_apply=%region_4.0 | all-reduce | flops 512 | bytes 4096 | tf_op jit(solution)/shard_map/psum | solution.py:20
  51.2 6.6 %all-reduce.1 = (f32[256]{0:T(256)S(1)}, f32[256]{0:T(256)S(1)}) all-reduce(f32[256]{0:T(256)S(1)} %get-tuple-element.15, f32[256]{0:T(256)S(1)} %get-tuple-element.16), channel_id=1, replica_groups=mesh['sp'=32,'tp_0'=4,'tp_1'=4] {'tp_1'}, use_global_device_ids=true, to_apply=%region_5.0 | all-reduce | flops 512 | bytes 4096 | tf_op jit(solution)/shard_map/psum | solution.py:20
  57.8 0.7 multiply_convert_fusion.1
  58.6 0.1 copy.34
  58.7 0.0 copy-start.5
  58.7 3.1 scatter_custom_fusion
  61.8 42.9 %all_to_all.31 = bf16[32,32,128]{2,1,0:T(8,128)(2,1)} all-to-all(bf16[32,32,128]{2,1,0:T(8,128)(2,1)S(1)} %bitcast.67), channel_id=1, replica_groups=mesh['sp'=32,'tp_0'=4,'tp_1'=4] {'sp'}, dimensions={0} | all-to-all | bytes 524288 | tf_op jit(solution)/shard_map/all_to_all | solution.py:126
  104.6 0.0 all-gather.3.cloned.1.call-update
  104.7 0.0 all-gather.5.cloned.1.call-start
  104.7 58.2 %all-gather.3.cloned.1.call-done = bf16[1024,2048]{1,0:T(8,128)(2,1)} async-done(((bf16[1024,128]{1,0:T(8,128)(2,1)}), bf16[1024,2048]{1,0:T(8,128)(2,1)}) %all-gather.3.cloned.1.call-update) | async-done | bytes 4194320 | tf_op jit(solution)/shard_map/all_gather | solution.py:134
  162.9 0.0 copy-done
  162.9 3.6 %convolution_minimum_fusion = f32[1024,256]{1,0:T(8,128)S(1)} fusion(bf16[1024,2048]{1,0:T(8,128)(2,1)} %all-gather.3.cloned.1.call-done, bf16[1,2048,256]{2,1,0:T(8,128)(2,1)S(1)} %copy-done), kind=kOutput, calls=%fused_computation.3 | convolution fusion | flops 1074003968 | bytes 6291456 | tf_op jit(solution)/shard_map/dot_general | solution.py:135
  166.5 0.0 copy-done.5
  166.5 0.0 copy-start.6
  166.5 2.2 fusion.3
  168.7 0.0 all-gather.5.cloned.1.call-update
  168.8 0.0 copy-start.2
  168.8 0.0 copy-start.1
  168.8 0.0 copy-start.3
  168.8 92.1 %all-gather.5.cloned.1.call-done = bf16[1024,4096]{1,0:T(8,128)(2,1)} async-done(((bf16[1024,256]{1,0:T(8,128)(2,1)}), bf16[1024,4096]{1,0:T(8,128)(2,1)}) %all-gather.5.cloned.1.call-update) | async-done | bytes 8388624 | tf_op jit(solution)/shard_map/all_gather | solution.py:64
  260.9 6.4 %convolution_convert_fusion = bf16[1024,128]{1,0:T(8,128)(2,1)} fusion(bf16[1024,4096]{1,0:T(8,128)(2,1)} %all-gather.5.cloned.1.call-done, bf16[1,4096,128]{2,1,0:T(8,128)(2,1)S(1)} %copy-done.6), kind=kOutput, calls=%fused_computation.9 | convolution fusion | flops 1073872896 | bytes 9699328 | tf_op jit(solution)/shard_map/dot_general | solution.py:63
  267.3 14.4 %all-to-all-start.3 = ((bf16[32,32,128]{2,1,0:T(8,128)(2,1)}), bf16[32,32,128]{2,1,0:T(8,128)(2,1)S(1)}, u32[]{:S(2)}, u32[]{:S(2)}) async-start(bf16[32,32,128]{2,1,0:T(8,128)(2,1)} %bitcast.15), calls=%async_computation.3 | async-start | bytes 524288 | tf_op jit(solution)/shard_map/all_to_all | solution.py:139
  281.7 0.1 copy.35
  281.9 22.1 %all-to-all-done.3 = bf16[32,32,128]{2,1,0:T(8,128)(2,1)S(1)} async-done(((bf16[32,32,128]{2,1,0:T(8,128)(2,1)}), bf16[32,32,128]{2,1,0:T(8,128)(2,1)S(1)}, u32[]{:S(2)}, u32[]{:S(2)}) %all-to-all-start.3) | async-done | bytes 262176 | tf_op jit(solution)/shard_map/all_to_all | solution.py:139
  304.0 1.3 gather_fusion
  305.3 0.4 fusion.8
  305.7 0.1 copy.36
  305.8 0.1 fusion.18
  306.0 8.1 %all-reduce.2 = (f32[256]{0:T(256)S(1)}, f32[256]{0:T(256)S(1)}) all-reduce(f32[256]{0:T(256)S(1)} %get-tuple-element.6, f32[256]{0:T(256)S(1)} %get-tuple-element.5), channel_id=1, replica_groups=mesh['sp'=32,'tp_0'=4,'tp_1'=4] {'tp_0'}, use_global_device_ids=true, to_apply=%region_15.16 | all-reduce | flops 512 | bytes 4096 | tf_op jit(solution)/shard_map/psum | solution.py:20
  314.1 6.5 %all-reduce = (f32[256]{0:T(256)S(1)}, f32[256]{0:T(256)S(1)}) all-reduce(f32[256]{0:T(256)S(1)} %get-tuple-element.13, f32[256]{0:T(256)S(1)} %get-tuple-element.14), channel_id=1, replica_groups=mesh['sp'=32,'tp_0'=4,'tp_1'=4] {'tp_1'}, use_global_device_ids=true, to_apply=%region_16.17 | all-reduce | flops 512 | bytes 4096 | tf_op jit(solution)/shard_map/psum | solution.py:20
  320.6 0.0 copy-done.3
  320.6 0.1 multiply_convert_fusion
  320.7 0.7 copy.37
  (14 shorter events, 0.1 us)
Async XLA Ops:
  6.5 156.3 %copy-start = (bf16[1,2048,256]{2,1,0:T(8,128)(2,1)S(1)}, bf16[1,2048,256]{2,1,0:T(8,128)(2,1)}, u32[]{:S(2)}) copy-start(bf16[1,2048,256]{2,1,0:T(8,128)(2,1)} %param.25) | copy-start | bytes 3145732
  7.4 20.1 %collective-permute-start = (f32[2]{0:T(128)S(1)}, f32[2]{0:T(128)S(1)}, u32[]{:S(2)}, u32[]{:S(2)}) collective-permute-start(f32[2]{0:T(128)S(1)} %slice.34), channel_id=1, source_target_pairs={{0,16},{16,32},{32,48},{48,64},{64,80},{80,96},{96,112},{112,128},... | collective-permute-start | bytes 32 | tf_op jit(solution)/shard_map/ppermute | solution.py:26
  13.1 15.2 %collective-permute-start.1 = (f32[2,32]{0,1:T(8,128)S(1)}, f32[2,32]{0,1:T(8,128)S(1)}, u32[]{:S(2)}, u32[]{:S(2)}) collective-permute-start(f32[2,32]{0,1:T(8,128)S(1)} %slice.48), channel_id=1, source_target_pairs={{0,16},{16,32},{32,48},{48,64},{64,80},{80,96},{96,112},{112,128},... | collective-permute-start | bytes 776 | tf_op jit(solution)/shard_map/ppermute | solution.py:26
  16.6 13.6 %all-to-all-start.1 = ((bf16[32,16,128]{2,0,1:T(8,128)(2,1)}), bf16[32,16,128]{2,0,1:T(8,128)(2,1)S(1)}, u32[]{:S(2)}, u32[]{:S(2)}) async-start(bf16[32,16,128]{2,0,1:T(8,128)(2,1)} %copy_bitcast_fusion), calls=%async_computation.1 | async-start | bytes 262144 | tf_op jit(solution)/shard_map/all_to_all | solution.py:101
  30.9 13.3 %all-to-all-start = ((bf16[16,256,32]{1,2,0:T(8,128)(2,1)}), bf16[16,256,32]{1,2,0:T(8,128)(2,1)S(1)}, u32[]{:S(2)}, u32[]{:S(2)}) async-start(bf16[16,256,32]{1,2,0:T(8,128)(2,1)} %broadcast_in_dim.4), calls=%async_computation | async-start | bytes 524288 | tf_op jit(solution)/shard_map/all_to_all | solution.py:37
  36.6 126.3 %all-gather.3.cloned.1.call-start = ((), (), s32[]{:S(2)}) async-start(), calls=%async_computation.4 | async-start | bytes 4456448 | tf_op jit(solution)/shard_map/all_gather | solution.py:134
  58.7 107.8 %copy-start.5 = (bf16[1,2048,256]{2,1,0:T(8,128)(2,1)S(1)}, bf16[1,2048,256]{2,1,0:T(8,128)(2,1)}, u32[]{:S(2)}) copy-start(bf16[1,2048,256]{2,1,0:T(8,128)(2,1)} %param.26) | copy-start | bytes 3145732
  104.7 156.3 %all-gather.5.cloned.1.call-start = ((), (), s32[]{:S(2)}) async-start(), calls=%async_computation.5 | async-start | bytes 8912896 | tf_op jit(solution)/shard_map/all_gather | solution.py:64
  162.9 3.6 %copy-start.4 = (bf16[1024,2048]{1,0:T(8,128)(2,1)S(1)}, bf16[1024,2048]{1,0:T(8,128)(2,1)}, u32[]{:S(2)}) copy-start(bf16[1024,2048]{1,0:T(8,128)(2,1)} %all-gather.3.cloned.1.call-done) | copy-start | bytes 12582916
  166.5 94.4 %copy-start.6 = (bf16[1,4096,128]{2,1,0:T(8,128)(2,1)S(1)}, bf16[1,4096,128]{2,1,0:T(8,128)(2,1)}, u32[]{:S(2)}) copy-start(bf16[1,4096,128]{2,1,0:T(8,128)(2,1)} %param.27) | copy-start | bytes 3145732
  168.8 112.9 %copy-start.2 = (f32[256,2]{0,1:T(2,128)S(1)}, f32[256,2]{0,1:T(2,128)}, u32[]{:S(2)}) copy-start(f32[256,2]{0,1:T(2,128)} %param.24) | copy-start | bytes 6148
  168.8 137.1 %copy-start.1 = (f32[128]{0:T(128)S(1)}, f32[128]{0:T(128)}, u32[]{:S(2)}) copy-start(f32[128]{0:T(128)} %param.21) | copy-start | bytes 1540
  168.8 151.8 %copy-start.3 = (f32[128]{0:T(128)S(1)}, f32[128]{0:T(128)}, u32[]{:S(2)}) copy-start(f32[128]{0:T(128)} %param.22) | copy-start | bytes 1540
  267.3 36.6 %all-to-all-start.3 = ((bf16[32,32,128]{2,1,0:T(8,128)(2,1)}), bf16[32,32,128]{2,1,0:T(8,128)(2,1)S(1)}, u32[]{:S(2)}, u32[]{:S(2)}) async-start(bf16[32,32,128]{2,1,0:T(8,128)(2,1)} %bitcast.15), calls=%async_computation.3 | async-start | bytes 524288 | tf_op jit(solution)/shard_map/all_to_all | solution.py:139
Sparse Core Ops, SparseCore 0:
  104.8 58.0 all-gather.2
  168.9 91.9 all-gather.4
where the time goes:
time: 332 us; the launch traced here: 328 us
  waiting for transfers between devices  180 us (54%)
  blocking collectives  70.8 us (21%)
  starting transfers between devices  33.7 us (10%)
  between operations  13.7 us (4%)
  matrix products  12.5 us (4%)
  local copies, waits for them, and re-layouts  11.3 us (3%)
  other arithmetic  6.58 us (2%)
    all_gather x1, waiting for transfers between devices, project_down(): lax.all_gather(hidden, TP, axis=1, tiled=True)  92.1 us
    all_gather x1, waiting for transfers between devices, per_device(): shard_piece = lax.all_gather(flat_rows, TP, axis=1, tiled=True)  58.2 us
    all_to_all x1, blocking collectives, per_device(): lax.all_to_all(send_buffer.reshape(expert_count, capacity, normed.shape[1...  42.9 us
    psum x4, blocking collectives, over_axes(): return functools.reduce(lax.psum, axes, value)  28 us
    all_to_all x1, waiting for transfers between devices, per_device(): lax.all_to_all(computed, 'sp', split_axis=0, concat_axis=0, tiled=True)  22.1 us
    all_to_all x1, starting transfers between devices, per_device(): lax.all_to_all(computed, 'sp', split_axis=0, concat_axis=0, tiled=True)  14.4 us
    ppermute x2, starting transfers between devices, from_behind(): lax.ppermute(value, axis, [(source, source + steps) for source in range(i...  6.82 us
    all_to_all x1, starting transfers between devices, per_device(): lax.all_to_all(out_weight, TP, split_axis=1, concat_axis=0, tiled=True)  6.75 us
  transfers between devices with their start and end apart: 7, of which 5 were waited for; matrix products, arithmetic and copies ran while one was open for 3% of the time, Pallas kernels for 0%

commit v1 on v0

v1 whole, which is shorter than its diff:
```python
import jax
import jax.numpy as jnp
from jax import lax
from jax.experimental import pallas as pl
from jax.experimental.pallas import tpu as pltpu
from jax.sharding import Mesh
from jax.sharding import PartitionSpec as P

D = 2048
CAP = 32
ALPHA = 8.0**0.25
EPSILON = 1e-05
LIMIT = 7.0
SLOPE = 1.702
MESH_ID = pl.DeviceIdType.MESH
BF = jnp.bfloat16
F32 = jnp.float32

NZ, NC, NY, NX = 16, 2, 4, 4
NSP = NZ * NC
ROWS = NSP * CAP
GROUPS = 4
GR = ROWS // GROUPS
HALF = GR // 2
QUARTER = HALF // 2
KPG = GR // CAP


def z_shift(k):
    step, side = k // 2, k % 2
    if step == 0:
        return 0, side
    return ((step + 1) // 2 if step % 2 else NZ - step // 2), side


SCHEDULE = [
    ("a0", 0), ("a0", 1), ("a1", 0), ("a1", 1), ("a2", 0), ("a0", 2), ("a2", 1), ("a1", 2),
    ("a3", 0), ("a0", 3), ("a1", 3), ("c", 0), ("a3", 1), ("a2", 2), ("r1", 0), ("c", 1),
    ("a3", 2), ("a2", 3), ("r2", 0), ("r1", 1), ("c", 2), ("a3", 3), ("r3", 0), ("r2", 1),
    ("r1", 2), ("c", 3), ("r4", 0), ("r3", 1), ("r2", 2), ("r1", 3), ("r4", 1), ("r3", 2),
    ("r2", 3), ("r4", 2), ("r3", 3), ("r4", 3),
]


def column_of(row_ref, size):
    eye = lax.broadcasted_iota(jnp.int32, (size, size), 0) == lax.broadcasted_iota(
        jnp.int32, (size, size), 1
    )
    row = jnp.broadcast_to(row_ref, (size, size))
    return jnp.sum(jnp.where(eye, row, 0.0), axis=1, keepdims=True)


def nt_dot(a, b, dims):
    return lax.dot_general(a, b, (dims, ((), ())), preferred_element_type=F32)


def kernel(
    og, ig, ci, taps, ow, res, doc, mg, fg, routes, rw, wg, wu, wdi,
    out,
    halo, co, wc, wd, st, sp0, sp1, sb, x4, p4, ra1, ra2, rb1, rb2, q, r21, r22, ob, ret, fst,
    nrm, hs, ows, cos, sts, st2s, wds, zs, rets, ags, rss,
):
    z, c = lax.axis_index("z"), lax.axis_index("c")
    y, x = lax.axis_index("y"), lax.axis_index("x")
    own = y * NX + x
    pending = []

    def send(src, dst, sems, index, target):
        copy = pltpu.make_async_remote_copy(
            src_ref=src,
            dst_ref=dst,
            send_sem=sems.at[(0,) + index],
            recv_sem=sems.at[(1,) + index],
            device_id=target,
            device_id_type=MESH_ID,
        )
        copy.start()
        pending.append(copy)

    def landed(dst, sems, index):
        pltpu.make_async_remote_copy(
            src_ref=dst,
            dst_ref=dst,
            send_sem=sems.at[(0,) + index],
            recv_sem=sems.at[(1,) + index],
            device_id=(z, c, y, lax.rem(x + 1, NX)),
            device_id_type=MESH_ID,
        ).wait_recv()

    def in_plane(p):
        return lax.rem(y + p // NX, NY), lax.rem(x + p % NX, NX)

    def from_plane(p):
        return lax.rem(y + NY - p // NX, NY), lax.rem(x + NX - p % NX, NX)

    def along_z(k):
        dz, dc = z_shift(k)
        return (lax.rem(z + dz, NZ), lax.rem(c + dc, NC), y, x)

    def back_z(k):
        dz, dc = z_shift(k)
        return (lax.rem(z + NZ - dz, NZ), lax.rem(c + NC - dc, NC), y, x)

    barrier = pltpu.get_barrier_semaphore()
    for p in range(1, NY * NX):
        py, px = in_plane(p)
        pl.semaphore_signal(barrier, inc=1, device_id=(z, c, py, px), device_id_type=MESH_ID)
    for k in range(1, NSP):
        pl.semaphore_signal(barrier, inc=1, device_id=along_z(k), device_id_type=MESH_ID)

    product = ig[...].astype(F32) * ci[...].astype(F32)
    marks = doc[...].astype(F32)
    halo[0, 0:32, :] = product[:, 128:256]
    halo[0, 32:40, :] = jnp.broadcast_to(marks[:, 128:256], (8, 128))
    tap = [column_of(taps[i : i + 1, :], 32) for i in range(3)]
    ids = lax.broadcasted_iota(jnp.int32, (NSP, 256), 0)
    hits = [(routes[i : i + 1, :] == ids).astype(F32) for i in range(2)]
    before = (
        lax.broadcasted_iota(jnp.int32, (256, 256), 0)
        < lax.broadcasted_iota(jnp.int32, (256, 256), 1)
    ).astype(F32)
    counts = jnp.dot(
        (hits[0] + hits[1]).astype(BF), before.astype(BF), preferred_element_type=F32
    )
    slots = lax.broadcasted_iota(jnp.int32, (ROWS, 256), 0)
    for i, chosen in ((0, sp0), (1, sp1)):
        rank = jnp.sum(hits[i] * counts, axis=0, keepdims=True).astype(jnp.int32)
        expert = routes[i : i + 1, :]
        ez = jnp.right_shift(expert, 1)
        ec = expert - 2 * ez
        dz = ez - z
        dz = jnp.where(dz < 0, dz + NZ, dz)
        dc = jnp.where(ec == c, 0, 1)
        step = jnp.where(dz == 0, 0, jnp.where(dz <= NZ // 2, 2 * dz - 1, 2 * (NZ - dz)))
        slot = (step * 2 + dc) * CAP + rank
        chosen[...] = jnp.where(slots == slot, 1.0, 0.0).astype(BF)

    pl.semaphore_wait(barrier, NY * NX - 1 + NSP - 1)

    send(halo.at[0], halo.at[1], hs, (0,), (lax.rem(z + c, NZ), 1 - c, y, x))
    for p in range(1, NY * NX):
        py, px = in_plane(p)
        there = py * NX + px
        send(
            ow.at[:, pl.ds(pl.multiple_of(there * 128, 128), 128)],
            wc.at[pl.ds(pl.multiple_of(own * 32, 32), 32), :],
            ows, (p,), (z, c, py, px),
        )
    wc[pl.ds(pl.multiple_of(own * 32, 32), 32), :] = ow[
        :, pl.ds(pl.multiple_of(own * 128, 128), 128)
    ]
    landed(halo.at[1], hs, (0,))
    first = jnp.where((z == 0) & (c == 0), 0.0, 1.0)
    lanes = lax.broadcasted_iota(jnp.int32, (32, 256), 1)
    lane_row = lax.broadcasted_iota(jnp.int32, (1, 256), 1)
    prior = halo[1, 0:32, :]
    prior_mark = halo[1, 32:33, :]
    prior_full = jnp.concatenate([prior, prior], axis=1)
    mark_full = jnp.concatenate([prior_mark, prior_mark], axis=1)
    mixed = tap[2] * product
    for shift in (1, 2):
        back = jnp.where(
            lanes < shift, pltpu.roll(prior_full, shift, 1), pltpu.roll(product, shift, 1)
        )
        back_mark = jnp.where(
            lane_row < shift, pltpu.roll(mark_full, shift, 1), pltpu.roll(marks, shift, 1)
        )
        same = jnp.where(back_mark == marks, 1.0, 0.0)
        same = jnp.where(lane_row < shift, same * first, same)
        mixed = mixed + (same * tap[2 - shift]) * back
    my_rows = pl.ds(pl.multiple_of(own * 32, 32), 32)
    co[my_rows, :] = (og[...].astype(F32) * mixed).astype(BF)
    for p in range(1, NY * NX):
        py, px = in_plane(p)
        send(co.at[my_rows, :], co.at[my_rows, :], cos, (p,), (z, c, py, px))
    stream_t = ALPHA * res[...].astype(F32).T

    def send_down(group):
        for p in group:
            py, px = in_plane(p)
            there = py * NX + px
            send(
                wdi.at[pl.ds(pl.multiple_of(there * 256, 256), 256), :],
                wd.at[:, pl.ds(pl.multiple_of(own * 128, 128), 128)],
                wds, (p,), (z, c, py, px),
            )

    wd[:, pl.ds(pl.multiple_of(own * 128, 128), 128)] = wdi[
        pl.ds(pl.multiple_of(own * 256, 256), 256), :
    ]
    for p in range(1, NY * NX):
        fy, fx = from_plane(p)
        rows = pl.ds(pl.multiple_of((fy * NX + fx) * 32, 32), 32)
        landed(wc.at[rows, :], ows, (p,))
    for p in range(1, NY * NX):
        fy, fx = from_plane(p)
        rows = pl.ds(pl.multiple_of((fy * NX + fx) * 32, 32), 32)
        landed(co.at[rows, :], cos, (p,))
    stream_t = stream_t + nt_dot(wc[...], co[...], ((0,), (0,)))

    def norm(stream, which, sems, gain_col):
        s1 = jnp.sum(stream, axis=0, keepdims=True)
        s2 = jnp.sum(stream * stream, axis=0, keepdims=True)
        sub = lax.broadcasted_iota(jnp.int32, (8, 256), 0)
        st[which, own] = jnp.where(sub == 0, s1, s2)
        for p in range(1, NY * NX):
            py, px = in_plane(p)
            send(st.at[which, own], st.at[which, own], sems, (p,), (z, c, py, px))
        if which == 0:
            send_down(range(1, NY * NX))
        for p in range(1, NY * NX):
            fy, fx = from_plane(p)
            landed(st.at[which, fy * NX + fx], sems, (p,))
        total = st[which, 0]
        for j in range(1, NY * NX):
            total = total + st[which, j]
        mean = total[0:1, :] / D
        spread = total[1:2, :] / D - mean * mean
        return (stream - mean) * lax.rsqrt(spread + EPSILON) * gain_col

    normed_t = norm(stream_t, 0, sts, column_of(mg[...], 128)).astype(BF)
    nrm[...] = normed_t

    for g in range(GROUPS):
        rows = pl.ds(g * GR, GR)
        chosen = sp0[rows, :] + sp1[rows, :]
        sb[rows, :] = nt_dot(chosen, normed_t, ((1,), (1,))).astype(BF)
        for k in range(g * KPG, (g + 1) * KPG):
            cut = pl.ds(k * CAP, CAP)
            if k == 0:
                x4[y, x, cut, :] = sb[cut, :]
            else:
                send(sb.at[cut, :], x4.at[y, x, cut, :], zs, (k,), along_z(k))
    for p in range(1, NY * NX):
        fy, fx = from_plane(p)
        cols = pl.ds(pl.multiple_of((fy * NX + fx) * 128, 128), 128)
        landed(wd.at[:, cols], wds, (p,))

    def ring(axis, step):
        if axis == "x":
            return (z, c, y, lax.rem(x + step + NX, NX))
        return (z, c, lax.rem(y + step + NY, NY), x)

    def spot(axis, step):
        return lax.rem((x if axis == "x" else y) + step + 4, 4)

    def span(g, half, part):
        start = g * GR + half * HALF
        if part == "lo":
            return pl.ds(start, QUARTER)
        if part == "hi":
            return pl.ds(start + QUARTER, QUARTER)
        return pl.ds(start, HALF)

    def slab(buf, g, half, phase, step, part=None):
        rows = span(g, half, part)
        if half == 0:
            if phase == 0:
                return buf.at[y, spot("x", step), rows, :]
            return buf.at[spot("y", step), :, rows, :]
        if phase == 0:
            return buf.at[spot("y", step), x, rows, :]
        return buf.at[:, spot("x", step), rows, :]

    def axis_of(half, phase):
        return "xy"[(half + phase) % 2]

    def ag_send(g, phase):
        for half in range(2):
            axis = axis_of(half, phase)
            base = half * 8 + phase * 4
            mine = slab(x4, g, half, phase, 0)
            send(mine, mine, ags, (g, base), ring(axis, 1))
            send(mine, mine, ags, (g, base + 1), ring(axis, -1))

    def ag_relay(g, phase):
        for half in range(2):
            axis = axis_of(half, phase)
            base = half * 8 + phase * 4
            landed(slab(x4, g, half, phase, -1), ags, (g, base))
            low = slab(x4, g, half, phase, -1, "lo")
            send(low, low, ags, (g, base + 2), ring(axis, 1))
            landed(slab(x4, g, half, phase, 1), ags, (g, base + 1))
            high = slab(x4, g, half, phase, 1, "hi")
            send(high, high, ags, (g, base + 3), ring(axis, -1))

    def ag_end(g, phase):
        for half in range(2):
            base = half * 8 + phase * 4
            landed(slab(x4, g, half, phase, 2, "lo"), ags, (g, base + 2))
            landed(slab(x4, g, half, phase, 2, "hi"), ags, (g, base + 3))

    def compute(g):
        rows = pl.ds(g * GR, GR)
        inputs = jnp.concatenate(
            [x4[b, a, rows, :] for b in range(NY) for a in range(NX)], axis=1
        )
        gate = jnp.minimum(jnp.dot(inputs, wg[...], preferred_element_type=F32), LIMIT)
        up = jnp.clip(jnp.dot(inputs, wu[...], preferred_element_type=F32), -LIMIT, LIMIT)
        hidden = ((up + 1.0) * gate * jax.nn.sigmoid(SLOPE * gate)).astype(BF)
        for b in range(NY):
            part = jnp.dot(
                hidden, wd[:, b * 512 : (b + 1) * 512], preferred_element_type=F32
            ).astype(BF)
            for a in range(NX):
                p4[b, a, rows, :] = part[:, a * 128 : (a + 1) * 128]

    first_in = (ra1, rb1)
    second_in = (ra2, rb2)

    def rs_first(g, phase):
        for half in range(2):
            axis = axis_of(half, 1 - phase)
            base = half * 8 + phase * 4
            for way, part in ((0, "lo"), (1, "hi")):
                if phase == 0:
                    src = slab(p4, g, half, 1, 2, part)
                    dst = first_in[half].at[g, way]
                else:
                    cut = pl.ds(way * QUARTER, QUARTER)
                    src = q.at[g, half, spot(axis, 2), cut, :]
                    dst = r21.at[g, half, way]
                send(src, dst, rss, (g, base + way), ring(axis, 1 - 2 * way))

    def rs_second(g, phase):
        for half in range(2):
            axis = axis_of(half, 1 - phase)
            base = half * 8 + phase * 4
            for way, part in ((0, "lo"), (1, "hi")):
                step = 1 - 2 * way
                if phase == 0:
                    came = first_in[half].at[g, way]
                    edge = slab(p4, g, half, 1, step, part)
                    whole = slab(p4, g, half, 1, step)
                    dst = second_in[half].at[g, way]
                else:
                    came = r21.at[g, half, way]
                    cut = pl.ds(way * QUARTER, QUARTER)
                    edge = q.at[g, half, spot(axis, step), cut, :]
                    whole = q.at[g, half, spot(axis, step)]
                    dst = r22.at[g, half, way]
                landed(came, rss, (g, base + way))
                edge[...] = (edge[...].astype(F32) + came[...].astype(F32)).astype(BF)
                send(whole, dst, rss, (g, base + 2 + way), ring(axis, step))

    def rs_end(g, phase):
        for half in range(2):
            base = half * 8 + phase * 4
            axis = axis_of(half, 1 - phase)
            for way in range(2):
                dst = (second_in[half] if phase == 0 else r22.at[:, half]).at[g, way]
                landed(dst, rss, (g, base + 2 + way))
            if phase == 0:
                mine = slab(p4, g, half, 1, 0)
                fwd, bwd = second_in[half].at[g, 0], second_in[half].at[g, 1]
                q[g, half] = (
                    mine[...].astype(F32) + fwd[...].astype(F32) + bwd[...].astype(F32)
                ).astype(BF)
            else:
                rows = span(g, half, None)
                ob[rows, :] = (
                    q[g, half, spot(axis, 0)].astype(F32)
                    + r22[g, half, 0].astype(F32)
                    + r22[g, half, 1].astype(F32)
                ).astype(BF)

    for stage, g in SCHEDULE:
        if stage == "a0":
            for k in range(g * KPG, (g + 1) * KPG):
                if k > 0:
                    landed(x4.at[y, x, pl.ds(k * CAP, CAP), :], zs, (k,))
            ag_send(g, 0)
        elif stage == "a1":
            ag_relay(g, 0)
        elif stage == "a2":
            ag_end(g, 0)
            ag_send(g, 1)
        elif stage == "a3":
            ag_relay(g, 1)
        elif stage == "c":
            ag_end(g, 1)
            compute(g)
            rs_first(g, 0)
        elif stage == "r1":
            rs_second(g, 0)
        elif stage == "r2":
            rs_end(g, 0)
            rs_first(g, 1)
        elif stage == "r3":
            rs_second(g, 1)
        else:
            rs_end(g, 1)
            for k in range(g * KPG, (g + 1) * KPG):
                cut = pl.ds(k * CAP, CAP)
                if k == 0:
                    ret[cut, :] = ob[cut, :]
                else:
                    send(ob.at[cut, :], ret.at[cut, :], rets, (k,), back_z(k))

    for k in range(1, NSP):
        landed(ret.at[pl.ds(k * CAP, CAP), :], rets, (k,))
    results = ret[...]
    ffn = rw[0:1, :] * nt_dot(results, sp0[...], ((0,), (0,)))
    ffn = ffn + rw[1:2, :] * nt_dot(results, sp1[...], ((0,), (0,)))
    second = ALPHA * nrm[...].astype(F32) + ffn
    out[...] = norm(second, 1, st2s, column_of(fg[...], 128)).T.astype(BF)
    for copy in pending:
        copy.wait_send()


def per_device(
    out_gate, in_gate, conv_input, conv_taps, out_weight, residual, document, mix_gain,
    ffn_gain, routes, route_weight, expert_gate, expert_up, expert_down,
):
    vmem = pl.BlockSpec(memory_space=pltpu.VMEM)
    dma = pltpu.SemaphoreType.DMA
    scratch = [
        pltpu.VMEM((2, 40, 128), F32),
        pltpu.VMEM((512, 256), BF),
        pltpu.VMEM((512, 128), BF),
        pltpu.VMEM((256, D), BF),
        pltpu.VMEM((2, 16, 8, 256), F32),
        pltpu.VMEM((ROWS, 256), BF),
        pltpu.VMEM((ROWS, 256), BF),
        pltpu.VMEM((ROWS, 128), BF),
        pltpu.VMEM((NY, NX, ROWS, 128), BF),
        pltpu.VMEM((NY, NX, ROWS, 128), BF),
        pltpu.VMEM((GROUPS, 2, 4, QUARTER, 128), BF),
        pltpu.VMEM((GROUPS, 2, 4, HALF, 128), BF),
        pltpu.VMEM((GROUPS, 2, 4, QUARTER, 128), BF),
        pltpu.VMEM((GROUPS, 2, 4, HALF, 128), BF),
        pltpu.VMEM((GROUPS, 2, 4, HALF, 128), BF),
        pltpu.VMEM((GROUPS, 2, 2, QUARTER, 128), BF),
        pltpu.VMEM((GROUPS, 2, 2, HALF, 128), BF),
        pltpu.VMEM((ROWS, 128), BF),
        pltpu.VMEM((ROWS, 128), BF),
        pltpu.VMEM((8, 128), F32),
        pltpu.VMEM((128, 256), BF),
        dma((2, 1)),
        dma((2, 16)),
        dma((2, 16)),
        dma((2, 16)),
        dma((2, 16)),
        dma((2, 16)),
        dma((2, NSP)),
        dma((2, NSP)),
        dma((2, GROUPS, 16)),
        dma((2, GROUPS, 16)),
    ]
    return pl.pallas_call(
        kernel,
        out_shape=jax.ShapeDtypeStruct((256, 128), BF),
        in_specs=[vmem] * 14,
        out_specs=vmem,
        scratch_shapes=scratch,
        compiler_params=pltpu.CompilerParams(
            collective_id=0, has_side_effects=True, vmem_limit_bytes=60 * 1024 * 1024
        ),
    )(
        out_gate.T, in_gate.T, conv_input.T, conv_taps, out_weight, residual,
        document[None, :], mix_gain[None, :], ffn_gain[None, :], routes.T, route_weight.T,
        expert_gate[0], expert_up[0], expert_down[0],
    )


def solution(mesh):
    torus = Mesh(mesh.devices.reshape(NZ, NC, NY, NX), ("z", "c", "y", "x"))
    sp, tp = ("z", "c"), ("y", "x")
    in_specs = (
        P(sp, tp), P(sp, tp), P(sp, tp), P(None, tp), P(tp, None), P(sp, tp), P(sp), P(tp),
        P(tp), P(sp, None), P(sp, None), P(sp, None, tp), P(sp, None, tp), P(sp, None, tp),
    )
    return jax.shard_map(
        per_device, mesh=torus, in_specs=in_specs, out_specs=P(sp, tp), check_vma=False
    )
```

time: 332 us -> 122 us (0.37)
  waiting for transfers between devices: 180 us -> 0 us
  Pallas kernels: 0 us -> 120 us
  blocking collectives: 70.8 us -> 0 us
  starting transfers between devices: 33.7 us -> 0 us
  between operations: 13.7 us -> 0.01 us
  matrix products: 12.5 us -> 0 us
  local copies, waits for them, and re-layouts: 11.3 us -> 1.47 us
  other arithmetic: 6.58 us -> 0 us
    all_gather x2 -> x0, waiting for transfers between devices: 150 us -> none  [the longest x1 92.1 us: project_down(): lax.all_gather(hidden, TP, axis=1, tiled=True)]
    pallas_call x0 -> x1, Pallas kernels: none -> 120 us  [per_device(): pl.pallas_call(kernel, out_shape=jax.ShapeDtypeStruct((256, 128), BF), in...]
    all_to_all x1 -> x0, blocking collectives: 42.9 us -> none  [per_device(): lax.all_to_all(send_buffer.reshape(expert_count, capacity, normed.shape[1...]
    all_to_all x3 -> x0, waiting for transfers between devices: 29.5 us -> none  [the longest x1 22.1 us: per_device(): lax.all_to_all(computed, 'sp', split_axis=0, concat_axis=0, tiled=True)]
    psum x4 -> x0, blocking collectives: 28 us -> none  [over_axes(): return functools.reduce(lax.psum, axes, value)]
    all_to_all x3 -> x0, starting transfers between devices: 26.8 us -> none  [the longest x1 14.4 us: per_device(): lax.all_to_all(computed, 'sp', split_axis=0, concat_axis=0, tiled=True)]
    dot_general x4 -> x0, matrix products: 12.5 us -> none  [the longest x1 6.42 us: project_down(): jnp.dot(lax.all_gather(hidden, TP, axis=1, tiled=True), weight_down, pref...]
    ppermute x2 -> x0, starting transfers between devices: 6.82 us -> none  [from_behind(): lax.ppermute(value, axis, [(source, source + steps) for source in range(i...]
  transfers between devices with their start and end apart: 7 -> 0, of which waited for: 5 -> 0; matrix products, arithmetic and copies ran while one was open for 3% -> 0% of each run, Pallas kernels for 0% -> 0%
where the time goes in v1:
time: 122 us
  Pallas kernels  120 us (98%)
  local copies, waits for them, and re-layouts  1.47 us (1%)
    pallas_call x1, Pallas kernels, per_device(): pl.pallas_call(kernel, out_shape=jax.ShapeDtypeStruct((256, 128), BF), in...  120 us

profile of v1, /device:TPU:1, one launch (start us, length us, event | category | flops | bytes accessed | tf_op | source)
XLA Modules:
  0.0 121.6 jit_solution(1512910019171355954)
XLA Ops:
  0.0 120.1 %shard_map.136 = bf16[256,128]{1,0:T(8,128)(2,1)} custom-call(bf16[32,256]{1,0:T(8,128)(2,1)} %bitcast.14, bf16[32,256]{1,0:T(8,128)(2,1)} %bitcast.15, bf16[32,256]{1,0:T(8,128)(2,1)} %bitcast.16, f32[3,32]{1,0:T(4,128)} %taps.1, bf16[32,2048]{1,0:T(8,128)(2,1)} %ow.1, bf16[256,128]{1,0:T(8,128)(2,1)} %res.1, s32[1,256]{1,0:T(1,128)} %bitcast.19, ...), custom_call_target="tpu_custom_call" | custom-call | tf_op jit(solution)/shard_map/pallas_call | solution.py:450
  120.1 1.5 %copy.16 = bf16[256,128]{1,0:T(8,128)(2,1)} copy(bf16[256,128]{1,0:T(8,128)(2,1)} %shard_map.136) | data formatting | bytes 131072

commit v2 on v1

v2 whole, which is shorter than its diff:
```python
import jax
import jax.numpy as jnp
from jax import lax
from jax.experimental import pallas as pl
from jax.experimental.pallas import tpu as pltpu
from jax.sharding import Mesh
from jax.sharding import PartitionSpec as P

D = 2048
CAP = 32
ALPHA = 8.0**0.25
EPSILON = 1e-05
LIMIT = 7.0
SLOPE = 1.702
MESH_ID = pl.DeviceIdType.MESH
BF = jnp.bfloat16
F32 = jnp.float32

NZ, NC, NY, NX = 16, 2, 4, 4
NSP = NZ * NC
ROWS = NSP * CAP
GROUPS = 4
GR = ROWS // GROUPS
HALF = GR // 2
QUARTER = HALF // 2
KPG = GR // CAP


def z_shift(k):
    step, side = k // 2, k % 2
    step = PERM[step // 4] * 4 + step % 4
    if step == 0:
        return 0, side
    return ((step + 1) // 2 if step % 2 else NZ - step // 2), side


PERM = (0, 2, 3, 1)
SCHEDULE = [
    ("a0", 0), ("a1", 0), ("a0", 1), ("a2", 0), ("a0", 2), ("a1", 1), ("a0", 3), ("a3", 0),
    ("a1", 3), ("a1", 2), ("a2", 1), ("a2", 2), ("a2", 3), ("c", 0), ("a3", 1), ("a3", 2),
    ("a3", 3), ("h1", 0), ("c", 1), ("c", 2), ("c", 3), ("d", 0), ("h1", 1), ("h1", 2),
    ("h1", 3), ("e1", 0), ("d", 1), ("d", 2), ("d", 3), ("e1", 1), ("e2", 0), ("e1", 2),
    ("e1", 3), ("e2", 1), ("e2", 2), ("e2", 3),
]


def column_of(row_ref, size):
    eye = lax.broadcasted_iota(jnp.int32, (size, size), 0) == lax.broadcasted_iota(
        jnp.int32, (size, size), 1
    )
    row = jnp.broadcast_to(row_ref, (size, size))
    return jnp.sum(jnp.where(eye, row, 0.0), axis=1, keepdims=True)


def nt_dot(a, b, dims):
    return lax.dot_general(a, b, (dims, ((), ())), preferred_element_type=F32)


def kernel(
    og, ig, ci, taps, ow, res, doc, mg, fg, routes, rw, wgh, wuh, wdh,
    out,
    wg, wu, wdi, halo, co, wc, wda, wdb, wra, wrb, st, sp0, sp1, sb, x4, h4, p4, r1, r2, ob, ret,
    nrm, ls, hs, ows, cos, sts, st2s, wds, zs, rets, ags, hds, rss,
):
    z, c = lax.axis_index("z"), lax.axis_index("c")
    y, x = lax.axis_index("y"), lax.axis_index("x")
    own = y * NX + x
    pending = []

    def send(src, dst, sems, index, target):
        copy = pltpu.make_async_remote_copy(
            src_ref=src,
            dst_ref=dst,
            send_sem=sems.at[(0,) + index],
            recv_sem=sems.at[(1,) + index],
            device_id=target,
            device_id_type=MESH_ID,
        )
        copy.start()
        pending.append(copy)

    def landed(dst, sems, index):
        pltpu.make_async_remote_copy(
            src_ref=dst,
            dst_ref=dst,
            send_sem=sems.at[(0,) + index],
            recv_sem=sems.at[(1,) + index],
            device_id=(z, c, y, lax.rem(x + 1, NX)),
            device_id_type=MESH_ID,
        ).wait_recv()

    def in_plane(p):
        return lax.rem(y + p // NX, NY), lax.rem(x + p % NX, NX)

    def from_plane(p):
        return lax.rem(y + NY - p // NX, NY), lax.rem(x + NX - p % NX, NX)

    def along_z(k):
        dz, dc = z_shift(k)
        return (lax.rem(z + dz, NZ), lax.rem(c + dc, NC), y, x)

    def back_z(k):
        dz, dc = z_shift(k)
        return (lax.rem(z + NZ - dz, NZ), lax.rem(c + NC - dc, NC), y, x)

    barrier = pltpu.get_barrier_semaphore()
    loads = [
        pltpu.make_async_copy(wdh, wdi, ls.at[0]),
        pltpu.make_async_copy(wgh, wg, ls.at[1]),
        pltpu.make_async_copy(wuh, wu, ls.at[2]),
    ]
    for load in loads:
        load.start()
    with jax.named_scope("signals"):
        for p in range(1, NY * NX):
            py, px = in_plane(p)
            pl.semaphore_signal(barrier, inc=1, device_id=(z, c, py, px), device_id_type=MESH_ID)
        for k in range(1, NSP):
            pl.semaphore_signal(barrier, inc=1, device_id=along_z(k), device_id_type=MESH_ID)

    with jax.named_scope("local"):
        product = ig[...].astype(F32) * ci[...].astype(F32)
        marks = doc[...].astype(F32)
        halo[0, 0:32, :] = product[:, 128:256]
        halo[0, 32:40, :] = jnp.broadcast_to(marks[:, 128:256], (8, 128))
        tap = [column_of(taps[i : i + 1, :], 32) for i in range(3)]
        ids = lax.broadcasted_iota(jnp.int32, (NSP, 256), 0)
        hits = [(routes[i : i + 1, :] == ids).astype(F32) for i in range(2)]
        before = (
            lax.broadcasted_iota(jnp.int32, (256, 256), 0)
            < lax.broadcasted_iota(jnp.int32, (256, 256), 1)
        ).astype(F32)
        counts = jnp.dot(
            (hits[0] + hits[1]).astype(BF), before.astype(BF), preferred_element_type=F32
        )
        slots = lax.broadcasted_iota(jnp.int32, (ROWS, 256), 0)
        for i, chosen in ((0, sp0), (1, sp1)):
            rank = jnp.sum(hits[i] * counts, axis=0, keepdims=True).astype(jnp.int32)
            expert = routes[i : i + 1, :]
            ez = jnp.right_shift(expert, 1)
            ec = expert - 2 * ez
            dz = ez - z
            dz = jnp.where(dz < 0, dz + NZ, dz)
            dc = jnp.where(ec == c, 0, 1)
            step = jnp.where(dz == 0, 0, jnp.where(dz <= NZ // 2, 2 * dz - 1, 2 * (NZ - dz)))
            block = jnp.right_shift(step, 2)
            place = jnp.zeros_like(block)
            for here, there in enumerate(PERM):
                place = jnp.where(block == there, here, place)
            step = place * 4 + (step - block * 4)
            slot = (step * 2 + dc) * CAP + rank
            chosen[...] = jnp.where(slots == slot, 1.0, 0.0).astype(BF)

    with jax.named_scope("entry"):
        pl.semaphore_wait(barrier, NY * NX - 1 + NSP - 1)

    with jax.named_scope("halo_send"):
        send(halo.at[0], halo.at[1], hs, (0,), (lax.rem(z + c, NZ), 1 - c, y, x))
        for p in range(1, NY * NX):
            py, px = in_plane(p)
            there = py * NX + px
            send(
                ow.at[:, pl.ds(pl.multiple_of(there * 128, 128), 128)],
                wc.at[pl.ds(pl.multiple_of(own * 32, 32), 32), :],
                ows, (p,), (z, c, py, px),
            )
        wc[pl.ds(pl.multiple_of(own * 32, 32), 32), :] = ow[
            :, pl.ds(pl.multiple_of(own * 128, 128), 128)
        ]
    with jax.named_scope("halo_wait"):
        landed(halo.at[1], hs, (0,))
    with jax.named_scope("conv"):
        first = jnp.where((z == 0) & (c == 0), 0.0, 1.0)
        lanes = lax.broadcasted_iota(jnp.int32, (32, 256), 1)
        lane_row = lax.broadcasted_iota(jnp.int32, (1, 256), 1)
        prior = halo[1, 0:32, :]
        prior_mark = halo[1, 32:33, :]
        prior_full = jnp.concatenate([prior, prior], axis=1)
        mark_full = jnp.concatenate([prior_mark, prior_mark], axis=1)
        mixed = tap[2] * product
        for shift in (1, 2):
            back = jnp.where(
                lanes < shift, pltpu.roll(prior_full, shift, 1), pltpu.roll(product, shift, 1)
            )
            back_mark = jnp.where(
                lane_row < shift, pltpu.roll(mark_full, shift, 1), pltpu.roll(marks, shift, 1)
            )
            same = jnp.where(back_mark == marks, 1.0, 0.0)
            same = jnp.where(lane_row < shift, same * first, same)
            mixed = mixed + (same * tap[2 - shift]) * back
        my_rows = pl.ds(pl.multiple_of(own * 32, 32), 32)
        co[my_rows, :] = (og[...].astype(F32) * mixed).astype(BF)
        for p in range(1, NY * NX):
            py, px = in_plane(p)
            send(co.at[my_rows, :], co.at[my_rows, :], cos, (p,), (z, c, py, px))
    with jax.named_scope("residual"):
        stream_t = ALPHA * res[...].astype(F32).T

    def ring(axis, step):
        if axis == "x":
            return (z, c, y, lax.rem(x + step + NX, NX))
        return (z, c, lax.rem(y + step + NY, NY), x)

    def spot(axis, step):
        return lax.rem((x if axis == "x" else y) + step + 4, 4)

    def down_rows(half, step, part=None):
        lead = spot("yx"[half], step)
        if half == 0:
            return wdi.at[lead] if part is None else wdi.at[lead, pl.ds(2 * part, 2)]
        return wdi.at[:, lead] if part is None else wdi.at[pl.ds(2 * part, 2), lead]

    def down_cols(half, step, part=None):
        cols = pl.ds(pl.multiple_of(spot("yx"[half], step) * 128, 128), 128)
        buf = (wda, wdb)[half]
        return buf.at[:, :, cols] if part is None else buf.at[pl.ds(2 * part, 2), :, cols]

    def down_first():
        loads[0].wait()
        for half in range(2):
            for way in range(2):
                step = 1 - 2 * way
                send(
                    down_rows(half, step), down_cols(half, 0), wds, (half * 6 + way,),
                    ring("yx"[half], step),
                )

    def down_relayed():
        for half in range(2):
            for way in range(2):
                send(
                    down_rows(half, 2, way), (wra, wrb)[half].at[way], wds,
                    (half * 6 + 2 + way,), ring("yx"[half], 1 - 2 * way),
                )

    def down_relay():
        for half in range(2):
            for way in range(2):
                step = 1 - 2 * way
                came = (wra, wrb)[half].at[way]
                landed(came, wds, (half * 6 + 2 + way,))
                send(
                    came, down_cols(half, -step, way), wds, (half * 6 + 4 + way,),
                    ring("yx"[half], step),
                )

    def down_end():
        for half in range(2):
            for way in range(2):
                step = 1 - 2 * way
                landed(down_cols(half, -step), wds, (half * 6 + way,))
                landed(down_cols(half, 2, way), wds, (half * 6 + 4 + way,))

    with jax.named_scope("down_first"):
        down_first()
        own_y = pl.ds(pl.multiple_of(y * 128, 128), 128)
        own_x = pl.ds(pl.multiple_of(x * 128, 128), 128)
        wda[:, :, own_y] = wdi[y]
        wdb[:, :, own_x] = wdi[:, x]
    with jax.named_scope("mix_wait"):
        for p in range(1, NY * NX):
            fy, fx = from_plane(p)
            rows = pl.ds(pl.multiple_of((fy * NX + fx) * 32, 32), 32)
            landed(wc.at[rows, :], ows, (p,))
        for p in range(1, NY * NX):
            fy, fx = from_plane(p)
            rows = pl.ds(pl.multiple_of((fy * NX + fx) * 32, 32), 32)
            landed(co.at[rows, :], cos, (p,))
    with jax.named_scope("mix_dot"):
        stream_t = stream_t + nt_dot(wc[...], co[...], ((0,), (0,)))

    def norm(stream, which, sems, gain_col):
        s1 = jnp.sum(stream, axis=0, keepdims=True)
        s2 = jnp.sum(stream * stream, axis=0, keepdims=True)
        sub = lax.broadcasted_iota(jnp.int32, (2, 256), 0)
        st[which, own] = jnp.where(sub == 0, s1, s2)
        for p in range(1, NY * NX):
            py, px = in_plane(p)
            send(st.at[which, own], st.at[which, own], sems, (p,), (z, c, py, px))
        if which == 0:
            down_relayed()
        for p in range(1, NY * NX):
            fy, fx = from_plane(p)
            landed(st.at[which, fy * NX + fx], sems, (p,))
        total = st[which, 0]
        for j in range(1, NY * NX):
            total = total + st[which, j]
        mean = total[0:1, :] / D
        spread = total[1:2, :] / D - mean * mean
        return (stream - mean) * lax.rsqrt(spread + EPSILON) * gain_col

    with jax.named_scope("norm_a"):
        normed_t = norm(stream_t, 0, sts, column_of(mg[...], 128)).astype(BF)
    nrm[...] = normed_t

    with jax.named_scope("dispatch"):
        for g in range(GROUPS):
            rows = pl.ds(g * GR, GR)
            chosen = sp0[rows, :] + sp1[rows, :]
            sb[rows, :] = nt_dot(chosen, normed_t, ((1,), (1,))).astype(BF)
            for k in range(g * KPG, (g + 1) * KPG):
                cut = pl.ds(k * CAP, CAP)
                if k == 0:
                    x4[y, x, cut, :] = sb[cut, :]
                else:
                    send(sb.at[cut, :], x4.at[y, x, cut, :], zs, (k,), along_z(k))
    with jax.named_scope("down_relay"):
        down_relay()

    def span(g, half, part):
        start = g * GR + half * HALF
        if part == "lo":
            return pl.ds(start, QUARTER)
        if part == "hi":
            return pl.ds(start + QUARTER, QUARTER)
        return pl.ds(start, HALF)

    def slab(buf, g, half, phase, step, part=None):
        rows = span(g, half, part)
        if half == 0:
            if phase == 0:
                return buf.at[y, spot("x", step), rows, :]
            return buf.at[spot("y", step), :, rows, :]
        if phase == 0:
            return buf.at[spot("y", step), x, rows, :]
        return buf.at[:, spot("x", step), rows, :]

    def axis_of(half, phase):
        return "xy"[(half + phase) % 2]

    def ag_send(g, phase):
        for half in range(2):
            axis = axis_of(half, phase)
            base = half * 8 + phase * 4
            mine = slab(x4, g, half, phase, 0)
            send(mine, mine, ags, (g, base), ring(axis, 1))
            send(mine, mine, ags, (g, base + 1), ring(axis, -1))

    def ag_relay(g, phase):
        for half in range(2):
            axis = axis_of(half, phase)
            base = half * 8 + phase * 4
            landed(slab(x4, g, half, phase, -1), ags, (g, base))
            low = slab(x4, g, half, phase, -1, "lo")
            send(low, low, ags, (g, base + 2), ring(axis, 1))
            landed(slab(x4, g, half, phase, 1), ags, (g, base + 1))
            high = slab(x4, g, half, phase, 1, "hi")
            send(high, high, ags, (g, base + 3), ring(axis, -1))

    def ag_end(g, phase):
        for half in range(2):
            base = half * 8 + phase * 4
            landed(slab(x4, g, half, phase, 2, "lo"), ags, (g, base + 2))
            landed(slab(x4, g, half, phase, 2, "hi"), ags, (g, base + 3))

    def expert_in(g):
        rows = pl.ds(g * GR, GR)
        inputs = jnp.concatenate(
            [x4[b, a, rows, :] for b in range(NY) for a in range(NX)], axis=1
        )
        gate = jnp.minimum(jnp.dot(inputs, wg[...], preferred_element_type=F32), LIMIT)
        up = jnp.clip(jnp.dot(inputs, wu[...], preferred_element_type=F32), -LIMIT, LIMIT)
        hidden = ((up + 1.0) * gate * jax.nn.sigmoid(SLOPE * gate)).astype(BF)
        for half in range(2):
            h4[spot("xy"[half], 0), span(g, half, None), :] = hidden[
                half * HALF : (half + 1) * HALF, :
            ]

    def hidden_at(g, half, step, part=None):
        return h4.at[spot("xy"[half], step), span(g, half, part), :]

    def hidden_send(g):
        for half in range(2):
            for way in range(2):
                mine = hidden_at(g, half, 0)
                send(mine, mine, hds, (g, half * 4 + way), ring("xy"[half], 1 - 2 * way))

    def hidden_relay(g):
        for half in range(2):
            for way, part in ((0, "lo"), (1, "hi")):
                step = 1 - 2 * way
                landed(hidden_at(g, half, -step), hds, (g, half * 4 + way))
                piece = hidden_at(g, half, -step, part)
                send(piece, piece, hds, (g, half * 4 + 2 + way), ring("xy"[half], step))

    def hidden_end(g):
        for half in range(2):
            for way, part in ((0, "lo"), (1, "hi")):
                landed(hidden_at(g, half, 2, part), hds, (g, half * 4 + 2 + way))

    def expert_out(g):
        for half in range(2):
            rows = span(g, half, None)
            inputs = jnp.concatenate([h4[b, rows, :] for b in range(4)], axis=1)
            weights = (wda, wdb)[half][...].reshape(1024, 512)
            part = jnp.dot(inputs, weights, preferred_element_type=F32).astype(BF)
            for b in range(4):
                p4[b, rows, :] = part[:, b * 128 : (b + 1) * 128]

    def part_at(g, half, step, part=None):
        return p4.at[spot("yx"[half], step), span(g, half, part), :]

    def sum_first(g):
        for half in range(2):
            for way, part in ((0, "lo"), (1, "hi")):
                send(
                    part_at(g, half, 2, part), r1.at[g, half, way], rss,
                    (g, half * 4 + way), ring("yx"[half], 1 - 2 * way),
                )

    def sum_second(g):
        for half in range(2):
            for way, part in ((0, "lo"), (1, "hi")):
                step = 1 - 2 * way
                landed(r1.at[g, half, way], rss, (g, half * 4 + way))
                edge = part_at(g, half, step, part)
                edge[...] = (edge[...].astype(F32) + r1[g, half, way].astype(F32)).astype(BF)
                send(
                    part_at(g, half, step), r2.at[g, half, way], rss,
                    (g, half * 4 + 2 + way), ring("yx"[half], step),
                )

    def sum_end(g):
        for half in range(2):
            for way in range(2):
                landed(r2.at[g, half, way], rss, (g, half * 4 + 2 + way))
            ob[span(g, half, None), :] = (
                part_at(g, half, 0)[...].astype(F32)
                + r2[g, half, 0].astype(F32)
                + r2[g, half, 1].astype(F32)
            ).astype(BF)

    for stage, g in SCHEDULE:
        with jax.named_scope(f"{stage}_{g}"):
            if stage == "a0":
                for k in range(g * KPG, (g + 1) * KPG):
                    if k > 0:
                        landed(x4.at[y, x, pl.ds(k * CAP, CAP), :], zs, (k,))
                ag_send(g, 0)
            elif stage == "a1":
                ag_relay(g, 0)
            elif stage == "a2":
                ag_end(g, 0)
                ag_send(g, 1)
            elif stage == "a3":
                ag_relay(g, 1)
            elif stage == "c":
                ag_end(g, 1)
                if g == 0:
                    loads[1].wait()
                    loads[2].wait()
                expert_in(g)
                hidden_send(g)
            elif stage == "h1":
                hidden_relay(g)
            elif stage == "d":
                hidden_end(g)
                if g == 0:
                    down_end()
                expert_out(g)
                sum_first(g)
            elif stage == "e1":
                sum_second(g)
            else:
                sum_end(g)
                for k in range(g * KPG, (g + 1) * KPG):
                    cut = pl.ds(k * CAP, CAP)
                    if k == 0:
                        ret[cut, :] = ob[cut, :]
                    else:
                        send(ob.at[cut, :], ret.at[cut, :], rets, (k,), back_z(k))

    with jax.named_scope("ret_wait"):
        for k in range(1, NSP):
            landed(ret.at[pl.ds(k * CAP, CAP), :], rets, (k,))
    with jax.named_scope("combine"):
        results = ret[...]
        ffn = rw[0:1, :] * nt_dot(results, sp0[...], ((0,), (0,)))
        ffn = ffn + rw[1:2, :] * nt_dot(results, sp1[...], ((0,), (0,)))
        second = ALPHA * nrm[...].astype(F32) + ffn
    with jax.named_scope("norm_b"):
        out[...] = norm(second, 1, st2s, column_of(fg[...], 128)).T.astype(BF)
    for copy in pending:
        copy.wait_send()


def per_device(
    out_gate, in_gate, conv_input, conv_taps, out_weight, residual, document, mix_gain,
    ffn_gain, routes, route_weight, expert_gate, expert_up, expert_down,
):
    vmem = pl.BlockSpec(memory_space=pltpu.VMEM)
    away = pl.BlockSpec(memory_space=pl.ANY)
    dma = pltpu.SemaphoreType.DMA
    scratch = [
        pltpu.VMEM((D, 256), BF),
        pltpu.VMEM((D, 256), BF),
        pltpu.VMEM((NY, NX, 256, 128), BF),
        pltpu.VMEM((2, 40, 128), F32),
        pltpu.VMEM((512, 256), BF),
        pltpu.VMEM((512, 128), BF),
        pltpu.VMEM((4, 256, 512), BF),
        pltpu.VMEM((4, 256, 512), BF),
        pltpu.VMEM((2, 2, 256, 128), BF),
        pltpu.VMEM((2, 2, 256, 128), BF),
        pltpu.VMEM((2, 16, 2, 256), F32),
        pltpu.VMEM((ROWS, 256), BF),
        pltpu.VMEM((ROWS, 256), BF),
        pltpu.VMEM((ROWS, 128), BF),
        pltpu.VMEM((NY, NX, ROWS, 128), BF),
        pltpu.VMEM((4, ROWS, 256), BF),
        pltpu.VMEM((4, ROWS, 128), BF),
        pltpu.VMEM((GROUPS, 2, 2, QUARTER, 128), BF),
        pltpu.VMEM((GROUPS, 2, 2, HALF, 128), BF),
        pltpu.VMEM((ROWS, 128), BF),
        pltpu.VMEM((ROWS, 128), BF),
        pltpu.VMEM((128, 256), BF),
        dma((3,)),
        dma((2, 1)),
        dma((2, 16)),
        dma((2, 16)),
        dma((2, 16)),
        dma((2, 16)),
        dma((2, 12)),
        dma((2, NSP)),
        dma((2, NSP)),
        dma((2, GROUPS, 16)),
        dma((2, GROUPS, 8)),
        dma((2, GROUPS, 8)),
    ]
    return pl.pallas_call(
        kernel,
        out_shape=jax.ShapeDtypeStruct((256, 128), BF),
        in_specs=[vmem] * 11 + [away] * 3,
        out_specs=vmem,
        scratch_shapes=scratch,
        compiler_params=pltpu.CompilerParams(
            collective_id=0, has_side_effects=True, vmem_limit_bytes=60 * 1024 * 1024
        ),
    )(
        out_gate.T, in_gate.T, conv_input.T, conv_taps, out_weight, residual,
        document[None, :], mix_gain[None, :], ffn_gain[None, :], routes.T, route_weight.T,
        expert_gate[0], expert_up[0], expert_down[0].reshape(NY, NX, 256, 128),
    )


def solution(mesh):
    torus = Mesh(mesh.devices.reshape(NZ, NC, NY, NX), ("z", "c", "y", "x"))
    sp, tp = ("z", "c"), ("y", "x")
    in_specs = (
        P(sp, tp), P(sp, tp), P(sp, tp), P(None, tp), P(tp, None), P(sp, tp), P(sp), P(tp),
        P(tp), P(sp, None), P(sp, None), P(sp, None, tp), P(sp, None, tp), P(sp, None, tp),
    )
    return jax.shard_map(
        per_device, mesh=torus, in_specs=in_specs, out_specs=P(sp, tp), check_vma=False
    )
```

time: 122 us -> 109 us (0.89)
  Pallas kernels: 120 us -> 107 us
    pallas_call x1, Pallas kernels: 120 us -> 107 us  [per_device(): pl.pallas_call(kernel, out_shape=jax.ShapeDtypeStruct((256, 128), BF), in...]
where the time goes in v2:
time: 109 us
  Pallas kernels  107 us (98%)
  local copies, waits for them, and re-layouts  1.47 us (1%)
    pallas_call x1, Pallas kernels, per_device(): pl.pallas_call(kernel, out_shape=jax.ShapeDtypeStruct((256, 128), BF), in...  107 us

profile of v2, /device:TPU:1, one launch (start us, length us, event | category | flops | bytes accessed | tf_op | source)
XLA Modules:
  0.0 108.9 jit_solution(14108257826724036106)
XLA Ops:
  0.0 107.4 %shard_map.136 = bf16[256,128]{1,0:T(8,128)(2,1)} custom-call(bf16[32,256]{1,0:T(8,128)(2,1)} %bitcast.14, bf16[32,256]{1,0:T(8,128)(2,1)} %bitcast.15, bf16[32,256]{1,0:T(8,128)(2,1)} %bitcast.16, f32[3,32]{1,0:T(4,128)} %taps.1, bf16[32,2048]{1,0:T(8,128)(2,1)} %ow.1, bf16[256,128]{1,0:T(8,128)(2,1)} %res.1, s32[1,256]{1,0:T(1,128)} %bitcast.19, ...), custom_call_target="tpu_custom_call" | custom-call | tf_op jit(solution)/shard_map/pallas_call | solution.py:530
  107.4 1.5 %copy.16 = bf16[256,128]{1,0:T(8,128)(2,1)} copy(bf16[256,128]{1,0:T(8,128)(2,1)} %shard_map.136) | data formatting | bytes 131072

commit v3 on v2

v3 whole, which is shorter than its diff:
```python
import jax
import jax.numpy as jnp
from jax import lax
from jax.experimental import pallas as pl
from jax.experimental.pallas import tpu as pltpu
from jax.sharding import Mesh
from jax.sharding import PartitionSpec as P

D = 2048
CAP = 32
ALPHA = 8.0**0.25
EPSILON = 1e-05
LIMIT = 7.0
SLOPE = 1.702
MESH_ID = pl.DeviceIdType.MESH
BF = jnp.bfloat16
F32 = jnp.float32

NZ, NC, NY, NX = 16, 2, 4, 4
NSP = NZ * NC
ROWS = NSP * CAP
SIZES = (2, 2, 4, 4, 2, 2)
GROUPS = len(SIZES)
STARTS = tuple(sum(SIZES[:g]) for g in range(GROUPS))
ORDER = tuple(range(16))
GATHER_DIRECT = ()
SUM_DIRECT = (5,)


def z_shift(k):
    step, side = k // 2, k % 2
    step = ORDER[step]
    if step == 0:
        return 0, side
    return ((step + 1) // 2 if step % 2 else NZ - step // 2), side


SCHEDULE = [
    ("a0", 0), ("a0", 1), ("a1", 0), ("a0", 2), ("a1", 1), ("a2", 0), ("a1", 2), ("a2", 1),
    ("a0", 3), ("a3", 0), ("a2", 2), ("a0", 4), ("a3", 1), ("a1", 3), ("c", 0), ("a0", 5),
    ("a3", 2), ("a1", 4), ("a2", 3), ("c", 1), ("a1", 5), ("h1", 0), ("c", 2), ("a2", 4),
    ("a3", 3), ("a2", 5), ("h1", 1), ("d", 0), ("h1", 2), ("a3", 4), ("c", 3), ("a3", 5),
    ("d", 1), ("e1", 0), ("d", 2), ("c", 4), ("h1", 3), ("c", 5), ("e1", 1), ("e2", 0), ("h1", 4),
    ("e1", 2), ("d", 3), ("e2", 1), ("d", 4), ("d", 5), ("e2", 2), ("e1", 3), ("e1", 4),
    ("e2", 5), ("e2", 3), ("e2", 4),
]


NAMES = (
    ["halo", "ow", "co0", "co1", "st0", "st1", "ret"]
    + [f"down{h}{n}" for h in range(2) for n in range(3)]
    + [f"z{g}" for g in range(GROUPS)]
    + [f"{n}{g}" for g in range(GROUPS) for n in ("x0d", "x0r", "x1d", "x1r", "hd", "hr", "sd", "sr")]
)
RECV = {name: i for i, name in enumerate(NAMES)}
SENT_NAMES = (
    ["halo", "ow", "co", "st0", "st1", "ret", "down0", "down1", "z"]
    + [f"{n}{g}" for g in range(GROUPS) for n in ("x0", "x1", "h", "s")]
)
SENT = {name: i for i, name in enumerate(SENT_NAMES)}


def column_of(row_ref, size):
    eye = lax.broadcasted_iota(jnp.int32, (size, size), 0) == lax.broadcasted_iota(
        jnp.int32, (size, size), 1
    )
    row = jnp.broadcast_to(row_ref, (size, size))
    return jnp.sum(jnp.where(eye, row, 0.0), axis=1, keepdims=True)


def nt_dot(a, b, dims):
    return lax.dot_general(a, b, (dims, ((), ())), preferred_element_type=F32)


def kernel(*refs):
    away, out, near = refs[:14], refs[14], refs[15:29]
    og, ig, ci, taps, ow, res, doc, mg, fg, routes, rw, wg, wu, wdi = near
    (
        halo, co, wc, wda, wdb, wra, wrb, st, sp0, sp1, sb, x4, h4, p4, r1, r2, ob, ret, nrm,
        load_sems, sent_sems, recv_sems,
    ) = refs[29:]
    z, c = lax.axis_index("z"), lax.axis_index("c")
    y, x = lax.axis_index("y"), lax.axis_index("x")
    own = y * NX + x

    def send(src, dst, sent, recv, target):
        pltpu.make_async_remote_copy(
            src_ref=src,
            dst_ref=dst,
            send_sem=sent_sems.at[SENT[sent]],
            recv_sem=recv_sems.at[RECV[recv]],
            device_id=target,
            device_id_type=MESH_ID,
        ).start()

    def landed(like, recv):
        pltpu.make_async_remote_copy(
            src_ref=like,
            dst_ref=like,
            send_sem=sent_sems.at[0],
            recv_sem=recv_sems.at[RECV[recv]],
            device_id=(z, c, y, lax.rem(x + 1, NX)),
            device_id_type=MESH_ID,
        ).wait_recv()

    def drained(like, sent):
        pltpu.make_async_remote_copy(
            src_ref=like,
            dst_ref=like,
            send_sem=sent_sems.at[SENT[sent]],
            recv_sem=recv_sems.at[0],
            device_id=(z, c, y, lax.rem(x + 1, NX)),
            device_id_type=MESH_ID,
        ).wait_send()

    def in_plane(p):
        return lax.rem(y + p // NX, NY), lax.rem(x + p % NX, NX)

    def from_plane(p):
        return lax.rem(y + NY - p // NX, NY), lax.rem(x + NX - p % NX, NX)

    def along_z(k):
        dz, dc = z_shift(k)
        return (lax.rem(z + dz, NZ), lax.rem(c + dc, NC), y, x)

    def back_z(k):
        dz, dc = z_shift(k)
        return (lax.rem(z + NZ - dz, NZ), lax.rem(c + NC - dc, NC), y, x)

    barrier = pltpu.get_barrier_semaphore()
    with jax.named_scope("signals"):
        for p in range(1, NY * NX):
            py, px = in_plane(p)
            pl.semaphore_signal(barrier, inc=1, device_id=(z, c, py, px), device_id_type=MESH_ID)
        for k in range(1, NSP):
            pl.semaphore_signal(barrier, inc=1, device_id=along_z(k), device_id_type=MESH_ID)

    loads = [
        pltpu.make_async_copy(far, here, load_sems.at[i])
        for i, (far, here) in enumerate(zip(away, near))
    ]
    for i in (9, 1, 2, 6, 3, 4, 0, 5, 7, 8, 10, 13, 11, 12):
        loads[i].start()

    with jax.named_scope("local"):
        for i in range(11):
            loads[i].wait()
        product = ig[...].astype(F32) * ci[...].astype(F32)
        marks = doc[...].astype(F32)
        halo[0, 0:32, :] = product[:, 128:256]
        halo[0, 32:40, :] = jnp.broadcast_to(marks[:, 128:256], (8, 128))
        tap = [column_of(taps[i : i + 1, :], 32) for i in range(3)]
        ids = lax.broadcasted_iota(jnp.int32, (NSP, 256), 0)
        hits = [(routes[i : i + 1, :] == ids).astype(F32) for i in range(2)]
        before = (
            lax.broadcasted_iota(jnp.int32, (256, 256), 0)
            < lax.broadcasted_iota(jnp.int32, (256, 256), 1)
        ).astype(F32)
        counts = jnp.dot(
            (hits[0] + hits[1]).astype(BF), before.astype(BF), preferred_element_type=F32
        )
        slots = lax.broadcasted_iota(jnp.int32, (ROWS, 256), 0)
        for i, chosen in ((0, sp0), (1, sp1)):
            rank = jnp.sum(hits[i] * counts, axis=0, keepdims=True).astype(jnp.int32)
            expert = routes[i : i + 1, :]
            ez = jnp.right_shift(expert, 1)
            ec = expert - 2 * ez
            dz = ez - z
            dz = jnp.where(dz < 0, dz + NZ, dz)
            dc = jnp.where(ec == c, 0, 1)
            step = jnp.where(dz == 0, 0, jnp.where(dz <= NZ // 2, 2 * dz - 1, 2 * (NZ - dz)))
            place = jnp.zeros_like(step)
            for here, there in enumerate(ORDER):
                place = jnp.where(step == there, here, place)
            step = place
            slot = (step * 2 + dc) * CAP + rank
            chosen[...] = jnp.where(slots == slot, 1.0, 0.0).astype(BF)

    with jax.named_scope("entry"):
        pl.semaphore_wait(barrier, NY * NX - 1 + NSP - 1)

    my_rows = pl.ds(pl.multiple_of(own * 32, 32), 32)

    def mix(before, before_mark, piece, mark):
        lanes = lax.broadcasted_iota(jnp.int32, (32, 128), 1)
        lane_row = lax.broadcasted_iota(jnp.int32, (1, 128), 1)
        mixed = tap[2] * piece
        for shift in (1, 2):
            back = jnp.where(
                lanes < shift, pltpu.roll(before, shift, 1), pltpu.roll(piece, shift, 1)
            )
            back_mark = jnp.where(
                lane_row < shift, pltpu.roll(before_mark, shift, 1), pltpu.roll(mark, shift, 1)
            )
            same = jnp.where(back_mark == mark, 1.0, 0.0)
            mixed = mixed + (same * tap[2 - shift]) * back
        return mixed

    def send_mixed(part):
        cols = pl.ds(part * 128, 128)
        for p in range(1, NY * NX):
            py, px = in_plane(p)
            send(co.at[my_rows, cols], co.at[my_rows, cols], "co", f"co{part}", (z, c, py, px))

    with jax.named_scope("halo_send"):
        send(halo.at[0], halo.at[1], "halo", "halo", (lax.rem(z + c, NZ), 1 - c, y, x))
        late = mix(product[:, 0:128], marks[:, 0:128], product[:, 128:256], marks[:, 128:256])
        co[my_rows, 128:256] = (og[:, 128:256].astype(F32) * late).astype(BF)
        send_mixed(1)
        for p in range(1, NY * NX):
            py, px = in_plane(p)
            there = py * NX + px
            send(
                ow.at[:, pl.ds(pl.multiple_of(there * 128, 128), 128)], wc.at[my_rows, :],
                "ow", "ow", (z, c, py, px),
            )
        wc[my_rows, :] = ow[:, pl.ds(pl.multiple_of(own * 128, 128), 128)]
    with jax.named_scope("halo_wait"):
        landed(halo.at[1], "halo")
    with jax.named_scope("conv"):
        first = jnp.where((z == 0) & (c == 0), 1.0, 0.0)
        prior_mark = halo[1, 32:33, :] * (1.0 - first) - first
        early = mix(halo[1, 0:32, :], prior_mark, product[:, 0:128], marks[:, 0:128])
        co[my_rows, 0:128] = (og[:, 0:128].astype(F32) * early).astype(BF)
        send_mixed(0)
    with jax.named_scope("residual"):
        stream_t = ALPHA * res[...].astype(F32).T

    def ring(axis, step):
        if axis == "x":
            return (z, c, y, lax.rem(x + step + NX, NX))
        return (z, c, lax.rem(y + step + NY, NY), x)

    def spot(axis, step):
        return lax.rem((x if axis == "x" else y) + step + 4, 4)

    def down_rows(half, step, part=None):
        lead = spot("yx"[half], step)
        if half == 0:
            return wdi.at[lead] if part is None else wdi.at[lead, pl.ds(2 * part, 2)]
        return wdi.at[:, lead] if part is None else wdi.at[pl.ds(2 * part, 2), lead]

    def down_cols(half, step, part=None):
        cols = pl.ds(pl.multiple_of(spot("yx"[half], step) * 128, 128), 128)
        buf = (wda, wdb)[half]
        return buf.at[:, :, cols] if part is None else buf.at[pl.ds(2 * part, 2), :, cols]

    def down_sends():
        loads[13].wait()
        for half in range(2):
            for way in range(2):
                send(
                    down_rows(half, 2, way), (wra, wrb)[half].at[way], f"down{half}",
                    f"down{half}0", ring("yx"[half], 1 - 2 * way),
                )
        for half in range(2):
            for way in range(2):
                step = 1 - 2 * way
                send(
                    down_rows(half, step), down_cols(half, 0), f"down{half}", f"down{half}1",
                    ring("yx"[half], step),
                )
        own_y = pl.ds(pl.multiple_of(y * 128, 128), 128)
        own_x = pl.ds(pl.multiple_of(x * 128, 128), 128)
        wda[:, :, own_y] = wdi[y]
        wdb[:, :, own_x] = wdi[:, x]

    def down_relay():
        for half in range(2):
            landed((wra, wrb)[half], f"down{half}0")
            for way in range(2):
                step = 1 - 2 * way
                send(
                    (wra, wrb)[half].at[way], down_cols(half, -step, way), f"down{half}",
                    f"down{half}2", ring("yx"[half], step),
                )

    def down_end():
        for half in range(2):
            buf = (wda, wdb)[half]
            landed(buf.at[:, :, pl.ds(0, 256)], f"down{half}1")
            landed(buf.at[:, :, pl.ds(0, 128)], f"down{half}2")

    with jax.named_scope("mix_wait"):
        landed(wc.at[pl.ds(0, 480), :], "ow")
        landed(co.at[pl.ds(0, 480), pl.ds(0, 128)], "co1")
        landed(co.at[pl.ds(0, 480), pl.ds(0, 128)], "co0")
    with jax.named_scope("mix_dot"):
        stream_t = stream_t + nt_dot(wc[...], co[...], ((0,), (0,)))

    def norm(stream, which, gain_col):
        s1 = jnp.sum(stream, axis=0, keepdims=True)
        s2 = jnp.sum(stream * stream, axis=0, keepdims=True)
        sub = lax.broadcasted_iota(jnp.int32, (2, 256), 0)
        st[which, own] = jnp.where(sub == 0, s1, s2)
        for p in range(1, NY * NX):
            py, px = in_plane(p)
            send(st.at[which, own], st.at[which, own], f"st{which}", f"st{which}", (z, c, py, px))
        if which == 0:
            down_sends()
        landed(st.at[which, pl.ds(0, 15)], f"st{which}")
        total = st[which, 0]
        for j in range(1, NY * NX):
            total = total + st[which, j]
        mean = total[0:1, :] / D
        spread = total[1:2, :] / D - mean * mean
        return (stream - mean) * lax.rsqrt(spread + EPSILON) * gain_col

    with jax.named_scope("norm_a"):
        normed_t = norm(stream_t, 0, column_of(mg[...], 128)).astype(BF)
    nrm[...] = normed_t

    def rows_of(g):
        return pl.ds(STARTS[g] * 64, SIZES[g] * 64)

    def ks_of(g):
        return range(STARTS[g] * 2, (STARTS[g] + SIZES[g]) * 2)

    with jax.named_scope("dispatch"):
        for g in range(GROUPS):
            rows = rows_of(g)
            chosen = sp0[rows, :] + sp1[rows, :]
            sb[rows, :] = nt_dot(chosen, normed_t, ((1,), (1,))).astype(BF)
            for k in ks_of(g):
                cut = pl.ds(k * CAP, CAP)
                if k == 0:
                    x4[y, x, cut, :] = sb[cut, :]
                else:
                    send(sb.at[cut, :], x4.at[y, x, cut, :], "z", f"z{g}", along_z(k))
    with jax.named_scope("down_relay"):
        down_relay()

    def span(g, half, part):
        length = SIZES[g] * 32
        start = STARTS[g] * 64 + half * length
        if part == "lo":
            return pl.ds(start, length // 2)
        if part == "hi":
            return pl.ds(start + length // 2, length // 2)
        return pl.ds(start, length)

    def slab(buf, g, half, phase, step, part=None):
        rows = span(g, half, part)
        if half == 0:
            if phase == 0:
                return buf.at[y, spot("x", step), rows, :]
            return buf.at[spot("y", step), :, rows, :]
        if phase == 0:
            return buf.at[spot("y", step), x, rows, :]
        return buf.at[:, spot("x", step), rows, :]

    def axis_of(half, phase):
        return "xy"[(half + phase) % 2]

    def steps_of(g, chosen):
        return (1, -1, 2) if g in chosen else (1, -1)

    def ag_like(g, phase, count):
        if phase == 0:
            return x4.at[0, pl.ds(0, count), rows_of(g), :]
        return x4.at[pl.ds(0, count), :, rows_of(g), :]

    def ag_send(g, phase):
        for half in range(2):
            for step in steps_of(g, GATHER_DIRECT):
                mine = slab(x4, g, half, phase, 0)
                send(mine, mine, f"x{phase}{g}", f"x{phase}d{g}", ring(axis_of(half, phase), step))

    def ag_relay(g, phase):
        landed(ag_like(g, phase, 2), f"x{phase}d{g}")
        for half in range(2):
            for step, part in ((1, "lo"), (-1, "hi")):
                piece = slab(x4, g, half, phase, -step, part)
                send(
                    piece, piece, f"x{phase}{g}", f"x{phase}r{g}", ring(axis_of(half, phase), step)
                )

    def ag_end(g, phase):
        if g in GATHER_DIRECT:
            landed(ag_like(g, phase, 3), f"x{phase}d{g}")
        else:
            landed(ag_like(g, phase, 1), f"x{phase}r{g}")

    def expert_in(g):
        rows = rows_of(g)
        inputs = jnp.concatenate(
            [x4[b, a, rows, :] for b in range(NY) for a in range(NX)], axis=1
        )
        gate = jnp.minimum(jnp.dot(inputs, wg[...], preferred_element_type=F32), LIMIT)
        up = jnp.clip(jnp.dot(inputs, wu[...], preferred_element_type=F32), -LIMIT, LIMIT)
        hidden = ((up + 1.0) * gate * jax.nn.sigmoid(SLOPE * gate)).astype(BF)
        for half in range(2):
            h4[spot("xy"[half], 0), span(g, half, None), :] = hidden[
                half * SIZES[g] * 32 : (half + 1) * SIZES[g] * 32, :
            ]

    def hidden_at(g, half, step, part=None):
        return h4.at[spot("xy"[half], step), span(g, half, part), :]

    def hidden_send(g):
        for half in range(2):
            for step in steps_of(g, SUM_DIRECT):
                mine = hidden_at(g, half, 0)
                send(mine, mine, f"h{g}", f"hd{g}", ring("xy"[half], step))

    def hidden_relay(g):
        landed(h4.at[pl.ds(0, 2), rows_of(g), :], f"hd{g}")
        for half in range(2):
            for step, part in ((1, "lo"), (-1, "hi")):
                piece = hidden_at(g, half, -step, part)
                send(piece, piece, f"h{g}", f"hr{g}", ring("xy"[half], step))

    def hidden_end(g):
        if g in SUM_DIRECT:
            landed(h4.at[pl.ds(0, 3), rows_of(g), :], f"hd{g}")
        else:
            landed(h4.at[pl.ds(0, 1), rows_of(g), :], f"hr{g}")

    def expert_out(g):
        for half in range(2):
            rows = span(g, half, None)
            inputs = jnp.concatenate([h4[b, rows, :] for b in range(4)], axis=1)
            weights = (wda, wdb)[half][...].reshape(1024, 512)
            part = jnp.dot(inputs, weights, preferred_element_type=F32).astype(BF)
            for b in range(4):
                p4[b, rows, :] = part[:, b * 128 : (b + 1) * 128]

    def part_at(g, half, step, part=None):
        return p4.at[spot("yx"[half], step), span(g, half, part), :]

    def first_at(g, half, way):
        return r1.at[half, way, pl.ds(STARTS[g] * 16, SIZES[g] * 16), :]

    def second_at(g, half, way):
        return r2.at[half, way, pl.ds(STARTS[g] * 32, SIZES[g] * 32), :]

    def sum_first(g):
        for half in range(2):
            axis = "yx"[half]
            if g in SUM_DIRECT:
                for way, step in enumerate(steps_of(g, SUM_DIRECT)):
                    send(
                        part_at(g, half, step), second_at(g, half, way), f"s{g}", f"sd{g}",
                        ring(axis, step),
                    )
            else:
                for way, part in ((0, "lo"), (1, "hi")):
                    send(
                        part_at(g, half, 2, part), first_at(g, half, way), f"s{g}", f"sr{g}",
                        ring(axis, 1 - 2 * way),
                    )

    def sum_second(g):
        landed(p4.at[pl.ds(0, 1), rows_of(g), :], f"sr{g}")
        for half in range(2):
            for way, part in ((0, "lo"), (1, "hi")):
                step = 1 - 2 * way
                edge = part_at(g, half, step, part)
                came = first_at(g, half, way)
                edge[...] = (edge[...].astype(F32) + came[...].astype(F32)).astype(BF)
                send(
                    part_at(g, half, step), second_at(g, half, way), f"s{g}", f"sd{g}",
                    ring("yx"[half], step),
                )

    def sum_end(g):
        ways = len(steps_of(g, SUM_DIRECT))
        landed(p4.at[pl.ds(0, ways), rows_of(g), :], f"sd{g}")
        for half in range(2):
            total = part_at(g, half, 0)[...].astype(F32)
            for way in range(ways):
                total = total + second_at(g, half, way)[...].astype(F32)
            ob[span(g, half, None), :] = total.astype(BF)

    for stage, g in SCHEDULE:
        with jax.named_scope(f"{stage}_{g}"):
            if stage == "a0":
                skip = CAP if g == 0 else 0
                arrived = pl.ds(STARTS[g] * 64 + skip, SIZES[g] * 64 - skip)
                landed(x4.at[y, x, arrived, :], f"z{g}")
                ag_send(g, 0)
            elif stage == "a1":
                ag_relay(g, 0)
            elif stage == "a2":
                ag_end(g, 0)
                ag_send(g, 1)
            elif stage == "a3":
                ag_relay(g, 1)
            elif stage == "c":
                ag_end(g, 1)
                if g == 0:
                    loads[11].wait()
                    loads[12].wait()
                expert_in(g)
                hidden_send(g)
            elif stage == "h1":
                hidden_relay(g)
            elif stage == "d":
                hidden_end(g)
                if g == 0:
                    down_end()
                expert_out(g)
                sum_first(g)
            elif stage == "e1":
                sum_second(g)
            else:
                sum_end(g)
                for k in ks_of(g):
                    cut = pl.ds(k * CAP, CAP)
                    if k == 0:
                        ret[cut, :] = ob[cut, :]
                    else:
                        send(ob.at[cut, :], ret.at[cut, :], "ret", "ret", back_z(k))

    with jax.named_scope("drain"):
        drained(halo.at[0], "halo")
        drained(wc.at[pl.ds(0, 480), :], "ow")
        drained(co.at[pl.ds(0, 480), :], "co")
        drained(st.at[0, pl.ds(0, 15)], "st0")
        drained(wda, "down0")
        drained(wdb, "down1")
        drained(sb.at[pl.ds(CAP, ROWS - CAP), :], "z")
        for g in range(GROUPS):
            drained(ag_like(g, 0, 3), f"x0{g}")
            drained(ag_like(g, 1, 3), f"x1{g}")
            drained(h4.at[pl.ds(0, 3), rows_of(g), :], f"h{g}")
            drained(p4.at[pl.ds(0, 3), rows_of(g), :], f"s{g}")
    with jax.named_scope("ret_wait"):
        landed(ret.at[pl.ds(CAP, ROWS - CAP), :], "ret")
    with jax.named_scope("combine"):
        results = ret[...]
        ffn = rw[0:1, :] * nt_dot(results, sp0[...], ((0,), (0,)))
        ffn = ffn + rw[1:2, :] * nt_dot(results, sp1[...], ((0,), (0,)))
        second = ALPHA * nrm[...].astype(F32) + ffn
    with jax.named_scope("norm_b"):
        out[...] = norm(second, 1, column_of(fg[...], 128)).T.astype(BF)
    drained(st.at[1, pl.ds(0, 15)], "st1")
    drained(ob.at[pl.ds(CAP, ROWS - CAP), :], "ret")


def per_device(
    out_gate, in_gate, conv_input, conv_taps, out_weight, residual, document, mix_gain,
    ffn_gain, routes, route_weight, expert_gate, expert_up, expert_down,
):
    args = (
        out_gate.T, in_gate.T, conv_input.T, conv_taps, out_weight, residual,
        document[None, :], mix_gain[None, :], ffn_gain[None, :], routes.T, route_weight.T,
        expert_gate[0], expert_up[0], expert_down[0].reshape(NY, NX, 256, 128),
    )
    dma = pltpu.SemaphoreType.DMA
    scratch = [pltpu.VMEM(arg.shape, arg.dtype) for arg in args] + [
        pltpu.VMEM((2, 40, 128), F32),
        pltpu.VMEM((512, 256), BF),
        pltpu.VMEM((512, 128), BF),
        pltpu.VMEM((4, 256, 512), BF),
        pltpu.VMEM((4, 256, 512), BF),
        pltpu.VMEM((2, 2, 256, 128), BF),
        pltpu.VMEM((2, 2, 256, 128), BF),
        pltpu.VMEM((2, 16, 2, 256), F32),
        pltpu.VMEM((ROWS, 256), BF),
        pltpu.VMEM((ROWS, 256), BF),
        pltpu.VMEM((ROWS, 128), BF),
        pltpu.VMEM((NY, NX, ROWS, 128), BF),
        pltpu.VMEM((4, ROWS, 256), BF),
        pltpu.VMEM((4, ROWS, 128), BF),
        pltpu.VMEM((2, 2, ROWS // 4, 128), BF),
        pltpu.VMEM((2, 3, ROWS // 2, 128), BF),
        pltpu.VMEM((ROWS, 128), BF),
        pltpu.VMEM((ROWS, 128), BF),
        pltpu.VMEM((128, 256), BF),
        dma((len(args),)),
        dma((len(SENT),)),
        dma((len(RECV),)),
    ]
    return pl.pallas_call(
        kernel,
        out_shape=jax.ShapeDtypeStruct((256, 128), BF),
        in_specs=[pl.BlockSpec(memory_space=pl.ANY)] * len(args),
        out_specs=pl.BlockSpec(memory_space=pltpu.VMEM),
        scratch_shapes=scratch,
        compiler_params=pltpu.CompilerParams(
            collective_id=0, has_side_effects=True, vmem_limit_bytes=60 * 1024 * 1024
        ),
    )(*args)


def solution(mesh):
    torus = Mesh(mesh.devices.reshape(NZ, NC, NY, NX), ("z", "c", "y", "x"))
    sp, tp = ("z", "c"), ("y", "x")
    in_specs = (
        P(sp, tp), P(sp, tp), P(sp, tp), P(None, tp), P(tp, None), P(sp, tp), P(sp), P(tp),
        P(tp), P(sp, None), P(sp, None), P(sp, None, tp), P(sp, None, tp), P(sp, None, tp),
    )
    return jax.shard_map(
        per_device, mesh=torus, in_specs=in_specs, out_specs=P(sp, tp), check_vma=False
    )
```

time: 109 us -> 99.3 us (0.911)
  Pallas kernels: 107 us -> 97.7 us
    pallas_call x1, Pallas kernels: 107 us -> 97.7 us  [per_device(): pl.pallas_call(kernel, out_shape=jax.ShapeDtypeStruct((256, 128), BF), in...]
where the time goes in v3:
time: 99.3 us; the launch traced here: 99.1 us
  Pallas kernels  97.7 us (98%)
  local copies, waits for them, and re-layouts  1.47 us (1%)
    pallas_call x1, Pallas kernels, per_device(): pl.pallas_call(kernel, out_shape=jax.ShapeDtypeStruct((256, 128), BF), in...  97.7 us

profile of v3, /device:TPU:1, one launch (start us, length us, event | category | flops | bytes accessed | tf_op | source)
XLA Modules:
  0.0 99.1 jit_solution(11918188432662807336)
XLA Ops:
  0.0 97.7 %shard_map.136 = bf16[256,128]{1,0:T(8,128)(2,1)} custom-call(bf16[32,256]{1,0:T(8,128)(2,1)} %bitcast.14, bf16[32,256]{1,0:T(8,128)(2,1)} %bitcast.15, bf16[32,256]{1,0:T(8,128)(2,1)} %bitcast.16, f32[3,32]{1,0:T(4,128)} %refs_3_.1, bf16[32,2048]{1,0:T(8,128)(2,1)} %refs_4_.1, bf16[256,128]{1,0:T(8,128)(2,1)} %refs_5_.1, s32[1,256]{1,0:T(1,128)} %bitcast.19, ...), custom_call_target="tpu_custom_call" | custom-call | tf_op jit(solution)/shard_map/pallas_call | solution.py:575
  97.7 1.5 %copy.16 = bf16[256,128]{1,0:T(8,128)(2,1)} copy(bf16[256,128]{1,0:T(8,128)(2,1)} %shard_map.136) | data formatting | bytes 131072

commit v4 on v3

--- a/solution.py
+++ b/solution.py
@@ -19,12 +19,12 @@
 NZ, NC, NY, NX = 16, 2, 4, 4
 NSP = NZ * NC
 ROWS = NSP * CAP
-SIZES = (2, 2, 4, 4, 2, 2)
+SIZES = (1, 1, 2, 3, 3, 3, 2, 1)
 GROUPS = len(SIZES)
 STARTS = tuple(sum(SIZES[:g]) for g in range(GROUPS))
 ORDER = tuple(range(16))
-GATHER_DIRECT = ()
-SUM_DIRECT = (5,)
+GATHER_DIRECT = (0,)
+SUM_DIRECT = (6, 7)
 
 
 def z_shift(k):
@@ -36,13 +36,14 @@
 
 
 SCHEDULE = [
-    ("a0", 0), ("a0", 1), ("a1", 0), ("a0", 2), ("a1", 1), ("a2", 0), ("a1", 2), ("a2", 1),
-    ("a0", 3), ("a3", 0), ("a2", 2), ("a0", 4), ("a3", 1), ("a1", 3), ("c", 0), ("a0", 5),
-    ("a3", 2), ("a1", 4), ("a2", 3), ("c", 1), ("a1", 5), ("h1", 0), ("c", 2), ("a2", 4),
-    ("a3", 3), ("a2", 5), ("h1", 1), ("d", 0), ("h1", 2), ("a3", 4), ("c", 3), ("a3", 5),
-    ("d", 1), ("e1", 0), ("d", 2), ("c", 4), ("h1", 3), ("c", 5), ("e1", 1), ("e2", 0), ("h1", 4),
-    ("e1", 2), ("d", 3), ("e2", 1), ("d", 4), ("d", 5), ("e2", 2), ("e1", 3), ("e1", 4),
-    ("e2", 5), ("e2", 3), ("e2", 4),
+    ("a0", 0), ("a0", 1), ("a0", 2), ("a0", 3), ("a1", 1), ("a1", 2), ("a2", 0), ("a0", 4),
+    ("a1", 3), ("a2", 2), ("a2", 1), ("a0", 5), ("a1", 4), ("a2", 3), ("c", 0), ("a0", 6),
+    ("a3", 2), ("a1", 5), ("a3", 1), ("a2", 4), ("a0", 7), ("a1", 6), ("h1", 0), ("a3", 3),
+    ("c", 2), ("a2", 5), ("c", 1), ("a1", 7), ("a3", 4), ("a2", 6), ("d", 0), ("c", 3), ("h1", 2),
+    ("a3", 5), ("h1", 1), ("a2", 7), ("c", 4), ("a3", 6), ("e1", 0), ("h1", 3), ("d", 2),
+    ("c", 5), ("d", 1), ("a3", 7), ("h1", 4), ("c", 6), ("e2", 0), ("e1", 2), ("d", 3), ("h1", 5),
+    ("c", 7), ("e1", 1), ("d", 4), ("e2", 2), ("e1", 3), ("d", 6), ("d", 5), ("e2", 1), ("e1", 4),
+    ("d", 7), ("e2", 3), ("e1", 5), ("e2", 6), ("e2", 4), ("e2", 7), ("e2", 5),
 ]
 
 
@@ -143,13 +144,65 @@
         loads[i].start()
 
     with jax.named_scope("local"):
-        for i in range(11):
+        for i in (1, 2, 6, 3, 0):
             loads[i].wait()
         product = ig[...].astype(F32) * ci[...].astype(F32)
         marks = doc[...].astype(F32)
         halo[0, 0:32, :] = product[:, 128:256]
         halo[0, 32:40, :] = jnp.broadcast_to(marks[:, 128:256], (8, 128))
         tap = [column_of(taps[i : i + 1, :], 32) for i in range(3)]
+
+    with jax.named_scope("entry"):
+        pl.semaphore_wait(barrier, NY * NX - 1 + NSP - 1)
+
+    my_rows = pl.ds(pl.multiple_of(own * 32, 32), 32)
+
+    def mix(before, before_mark, piece, mark):
+        lanes = lax.broadcasted_iota(jnp.int32, (32, 128), 1)
+        lane_row = lax.broadcasted_iota(jnp.int32, (1, 128), 1)
+        mixed = tap[2] * piece
+        for shift in (1, 2):
+            back = jnp.where(
+                lanes < shift, pltpu.roll(before, shift, 1), pltpu.roll(piece, shift, 1)
+            )
+            back_mark = jnp.where(
+                lane_row < shift, pltpu.roll(before_mark, shift, 1), pltpu.roll(mark, shift, 1)
+            )
+            same = jnp.where(back_mark == mark, 1.0, 0.0)
+            mixed = mixed + (same * tap[2 - shift]) * back
+        return mixed
+
+    def send_mixed(part):
+        cols = pl.ds(part * 128, 128)
+        for p in range(1, NY * NX):
+            py, px = in_plane(p)
+            send(co.at[my_rows, cols], co.at[my_rows, cols], "co", f"co{part}", (z, c, py, px))
+
+    with jax.named_scope("halo_send"):
+        send(halo.at[0], halo.at[1], "halo", "halo", (lax.rem(z + c, NZ), 1 - c, y, x))
+        late = mix(product[:, 0:128], marks[:, 0:128], product[:, 128:256], marks[:, 128:256])
+        co[my_rows, 128:256] = (og[:, 128:256].astype(F32) * late).astype(BF)
+        send_mixed(1)
+        loads[4].wait()
+        for p in range(1, NY * NX):
+            py, px = in_plane(p)
+            there = py * NX + px
+            send(
+                ow.at[:, pl.ds(pl.multiple_of(there * 128, 128), 128)], wc.at[my_rows, :],
+                "ow", "ow", (z, c, py, px),
+            )
+        wc[my_rows, :] = ow[:, pl.ds(pl.multiple_of(own * 128, 128), 128)]
+    with jax.named_scope("halo_wait"):
+        landed(halo.at[1], "halo")
+    with jax.named_scope("conv"):
+        first = jnp.where((z == 0) & (c == 0), 1.0, 0.0)
+        prior_mark = halo[1, 32:33, :] * (1.0 - first) - first
+        early = mix(halo[1, 0:32, :], prior_mark, product[:, 0:128], marks[:, 0:128])
+        co[my_rows, 0:128] = (og[:, 0:128].astype(F32) * early).astype(BF)
+        send_mixed(0)
+    with jax.named_scope("slots"):
+        for i in (5, 7, 8, 9, 10):
+            loads[i].wait()
         ids = lax.broadcasted_iota(jnp.int32, (NSP, 256), 0)
         hits = [(routes[i : i + 1, :] == ids).astype(F32) for i in range(2)]
         before = (
@@ -175,54 +228,6 @@
             step = place
             slot = (step * 2 + dc) * CAP + rank
             chosen[...] = jnp.where(slots == slot, 1.0, 0.0).astype(BF)
-
-    with jax.named_scope("entry"):
-        pl.semaphore_wait(barrier, NY * NX - 1 + NSP - 1)
-
-    my_rows = pl.ds(pl.multiple_of(own * 32, 32), 32)
-
-    def mix(before, before_mark, piece, mark):
-        lanes = lax.broadcasted_iota(jnp.int32, (32, 128), 1)
-        lane_row = lax.broadcasted_iota(jnp.int32, (1, 128), 1)
-        mixed = tap[2] * piece
-        for shift in (1, 2):
-            back = jnp.where(
-                lanes < shift, pltpu.roll(before, shift, 1), pltpu.roll(piece, shift, 1)
-            )
-            back_mark = jnp.where(
-                lane_row < shift, pltpu.roll(before_mark, shift, 1), pltpu.roll(mark, shift, 1)
-            )
-            same = jnp.where(back_mark == mark, 1.0, 0.0)
-            mixed = mixed + (same * tap[2 - shift]) * back
-        return mixed
-
-    def send_mixed(part):
-        cols = pl.ds(part * 128, 128)
-        for p in range(1, NY * NX):
-            py, px = in_plane(p)
-            send(co.at[my_rows, cols], co.at[my_rows, cols], "co", f"co{part}", (z, c, py, px))
-
-    with jax.named_scope("halo_send"):
-        send(halo.at[0], halo.at[1], "halo", "halo", (lax.rem(z + c, NZ), 1 - c, y, x))
-        late = mix(product[:, 0:128], marks[:, 0:128], product[:, 128:256], marks[:, 128:256])
-        co[my_rows, 128:256] = (og[:, 128:256].astype(F32) * late).astype(BF)
-        send_mixed(1)
-        for p in range(1, NY * NX):
-            py, px = in_plane(p)
-            there = py * NX + px
-            send(
-                ow.at[:, pl.ds(pl.multiple_of(there * 128, 128), 128)], wc.at[my_rows, :],
-                "ow", "ow", (z, c, py, px),
-            )
-        wc[my_rows, :] = ow[:, pl.ds(pl.multiple_of(own * 128, 128), 128)]
-    with jax.named_scope("halo_wait"):
-        landed(halo.at[1], "halo")
-    with jax.named_scope("conv"):
-        first = jnp.where((z == 0) & (c == 0), 1.0, 0.0)
-        prior_mark = halo[1, 32:33, :] * (1.0 - first) - first
-        early = mix(halo[1, 0:32, :], prior_mark, product[:, 0:128], marks[:, 0:128])
-        co[my_rows, 0:128] = (og[:, 0:128].astype(F32) * early).astype(BF)
-        send_mixed(0)
     with jax.named_scope("residual"):
         stream_t = ALPHA * res[...].astype(F32).T
 
@@ -547,6 +552,7 @@
         document[None, :], mix_gain[None, :], ffn_gain[None, :], routes.T, route_weight.T,
         expert_gate[0], expert_up[0], expert_down[0].reshape(NY, NX, 256, 128),
     )
+    args = tuple(pltpu.with_memory_space_constraint(arg, pltpu.HBM) for arg in args)
     dma = pltpu.SemaphoreType.DMA
     scratch = [pltpu.VMEM(arg.shape, arg.dtype) for arg in args] + [
         pltpu.VMEM((2, 40, 128), F32),
@@ -579,7 +585,7 @@
         out_specs=pl.BlockSpec(memory_space=pltpu.VMEM),
         scratch_shapes=scratch,
         compiler_params=pltpu.CompilerParams(
-            collective_id=0, has_side_effects=True, vmem_limit_bytes=60 * 1024 * 1024
+            collective_id=0, has_side_effects=True, vmem_limit_bytes=48 * 1024 * 1024
         ),
     )(*args)
 

time: 99.3 us -> 95.4 us (0.961)
  Pallas kernels: 97.7 us -> 94.6 us
    pallas_call x1, Pallas kernels: 97.7 us -> 94.6 us  [per_device(): pl.pallas_call(kernel, out_shape=jax.ShapeDtypeStruct((256, 128), BF), in...]
where the time goes in v4:
time: 95.4 us; the launch traced here: 95.3 us
  Pallas kernels  94.6 us (99%)
    pallas_call x1, Pallas kernels, per_device(): pl.pallas_call(kernel, out_shape=jax.ShapeDtypeStruct((256, 128), BF), in...  94.6 us

profile of v4, /device:TPU:1, one launch (start us, length us, event | category | flops | bytes accessed | tf_op | source)
XLA Modules:
  0.0 95.3 jit_solution(7953378512703096848)
XLA Ops:
  0.0 94.6 %shard_map.136 = bf16[256,128]{1,0:T(8,128)(2,1)S(1)} custom-call(bf16[32,256]{1,0:T(8,128)(2,1)} %bitcast.14, bf16[32,256]{1,0:T(8,128)(2,1)} %bitcast.15, bf16[32,256]{1,0:T(8,128)(2,1)} %bitcast.16, f32[3,32]{1,0:T(4,128)} %refs_3_.1, bf16[32,2048]{1,0:T(8,128)(2,1)} %refs_4_.1, bf16[256,128]{1,0:T(8,128)(2,1)} %refs_5_.1, s32[1,256]{1,0:T(1,128)} %bitcast.19, ...), custom_call_target="tpu_custom_call" | custom-call | tf_op jit(solution)/shard_map/pallas_call | solution.py:581
  94.7 0.6 copy.16

commit v5 on v4

--- a/solution.py
+++ b/solution.py
@@ -19,12 +19,12 @@
 NZ, NC, NY, NX = 16, 2, 4, 4
 NSP = NZ * NC
 ROWS = NSP * CAP
-SIZES = (1, 1, 2, 3, 3, 3, 2, 1)
+SIZES = (1, 2, 4, 4, 2, 2, 1)
 GROUPS = len(SIZES)
 STARTS = tuple(sum(SIZES[:g]) for g in range(GROUPS))
 ORDER = tuple(range(16))
 GATHER_DIRECT = (0,)
-SUM_DIRECT = (6, 7)
+SUM_DIRECT = (5, 6)
 
 
 def z_shift(k):
@@ -36,14 +36,13 @@
 
 
 SCHEDULE = [
-    ("a0", 0), ("a0", 1), ("a0", 2), ("a0", 3), ("a1", 1), ("a1", 2), ("a2", 0), ("a0", 4),
-    ("a1", 3), ("a2", 2), ("a2", 1), ("a0", 5), ("a1", 4), ("a2", 3), ("c", 0), ("a0", 6),
-    ("a3", 2), ("a1", 5), ("a3", 1), ("a2", 4), ("a0", 7), ("a1", 6), ("h1", 0), ("a3", 3),
-    ("c", 2), ("a2", 5), ("c", 1), ("a1", 7), ("a3", 4), ("a2", 6), ("d", 0), ("c", 3), ("h1", 2),
-    ("a3", 5), ("h1", 1), ("a2", 7), ("c", 4), ("a3", 6), ("e1", 0), ("h1", 3), ("d", 2),
-    ("c", 5), ("d", 1), ("a3", 7), ("h1", 4), ("c", 6), ("e2", 0), ("e1", 2), ("d", 3), ("h1", 5),
-    ("c", 7), ("e1", 1), ("d", 4), ("e2", 2), ("e1", 3), ("d", 6), ("d", 5), ("e2", 1), ("e1", 4),
-    ("d", 7), ("e2", 3), ("e1", 5), ("e2", 6), ("e2", 4), ("e2", 7), ("e2", 5),
+    ("a0", 1), ("a0", 0), ("a0", 2), ("a1", 1), ("a2", 0), ("a1", 2), ("a0", 4), ("a0", 3),
+    ("a2", 2), ("a0", 5), ("a1", 4), ("a1", 3), ("a0", 6), ("a1", 5), ("a2", 4), ("a2", 3),
+    ("a2", 1), ("a1", 6), ("a2", 5), ("a3", 2), ("a3", 4), ("c", 0), ("a2", 6), ("a3", 5),
+    ("a3", 3), ("a3", 1), ("a3", 6), ("c", 4), ("c", 5), ("c", 3), ("h1", 4), ("c", 6), ("c", 2),
+    ("h1", 3), ("d", 5), ("c", 1), ("d", 4), ("h1", 2), ("d", 6), ("h1", 0), ("d", 3), ("h1", 1),
+    ("e2", 5), ("e1", 4), ("d", 2), ("d", 0), ("e2", 6), ("e1", 3), ("d", 1), ("e2", 4),
+    ("e1", 2), ("e2", 3), ("e1", 0), ("e1", 1), ("e2", 2), ("e2", 0), ("e2", 1),
 ]
 
 
@@ -365,11 +364,18 @@
             return x4.at[0, pl.ds(0, count), rows_of(g), :]
         return x4.at[pl.ds(0, count), :, rows_of(g), :]
 
-    def ag_send(g, phase):
+    def ag_send(g):
         for half in range(2):
             for step in steps_of(g, GATHER_DIRECT):
-                mine = slab(x4, g, half, phase, 0)
-                send(mine, mine, f"x{phase}{g}", f"x{phase}d{g}", ring(axis_of(half, phase), step))
+                mine = slab(x4, g, half, 0, 0)
+                send(mine, mine, f"x0{g}", f"x0d{g}", ring(axis_of(half, 0), step))
+
+    def ag_onward(g, places):
+        for place in places:
+            for half in range(2):
+                for step in steps_of(g, GATHER_DIRECT):
+                    piece = slab(x4, g, half, 0, place)
+                    send(piece, piece, f"x1{g}", f"x1d{g}", ring(axis_of(half, 1), step))
 
     def ag_relay(g, phase):
         landed(ag_like(g, phase, 2), f"x{phase}d{g}")
@@ -477,23 +483,26 @@
                 total = total + second_at(g, half, way)[...].astype(F32)
             ob[span(g, half, None), :] = total.astype(BF)
 
+    first_of = {stage: g for stage, g in reversed(SCHEDULE)}
     for stage, g in SCHEDULE:
         with jax.named_scope(f"{stage}_{g}"):
             if stage == "a0":
                 skip = CAP if g == 0 else 0
                 arrived = pl.ds(STARTS[g] * 64 + skip, SIZES[g] * 64 - skip)
                 landed(x4.at[y, x, arrived, :], f"z{g}")
-                ag_send(g, 0)
+                ag_send(g)
+                ag_onward(g, (0,))
             elif stage == "a1":
                 ag_relay(g, 0)
+                ag_onward(g, (-1, 1))
             elif stage == "a2":
                 ag_end(g, 0)
-                ag_send(g, 1)
+                ag_onward(g, (-1, 1, 2) if g in GATHER_DIRECT else (2,))
             elif stage == "a3":
                 ag_relay(g, 1)
             elif stage == "c":
                 ag_end(g, 1)
-                if g == 0:
+                if g == first_of["c"]:
                     loads[11].wait()
                     loads[12].wait()
                 expert_in(g)
@@ -502,7 +511,7 @@
                 hidden_relay(g)
             elif stage == "d":
                 hidden_end(g)
-                if g == 0:
+                if g == first_of["d"]:
                     down_end()
                 expert_out(g)
                 sum_first(g)

time: 95.4 us -> 93 us (0.975)
  Pallas kernels: 94.6 us -> 92.2 us
    pallas_call x1, Pallas kernels: 94.6 us -> 92.2 us  [per_device(): pl.pallas_call(kernel, out_shape=jax.ShapeDtypeStruct((256, 128), BF), in...]
where the time goes in v5:
time: 93 us; the launch traced here: 92.8 us
  Pallas kernels  92.2 us (99%)
    pallas_call x1, Pallas kernels, per_device(): pl.pallas_call(kernel, out_shape=jax.ShapeDtypeStruct((256, 128), BF), in...  92.2 us

profile of v5, /device:TPU:1, one launch (start us, length us, event | category | flops | bytes accessed | tf_op | source)
XLA Modules:
  0.0 92.8 jit_solution(2905680773975647738)
XLA Ops:
  0.0 92.2 %shard_map.136 = bf16[256,128]{1,0:T(8,128)(2,1)S(1)} custom-call(bf16[32,256]{1,0:T(8,128)(2,1)} %bitcast.14, bf16[32,256]{1,0:T(8,128)(2,1)} %bitcast.15, bf16[32,256]{1,0:T(8,128)(2,1)} %bitcast.16, f32[3,32]{1,0:T(4,128)} %refs_3_.1, bf16[32,2048]{1,0:T(8,128)(2,1)} %refs_4_.1, bf16[256,128]{1,0:T(8,128)(2,1)} %refs_5_.1, s32[1,256]{1,0:T(1,128)} %bitcast.19, ...), custom_call_target="tpu_custom_call" | custom-call | tf_op jit(solution)/shard_map/pallas_call | solution.py:590
  92.2 0.6 copy.16

commit v6 on v5

--- a/solution.py
+++ b/solution.py
@@ -46,6 +46,9 @@
 ]
 
 
+PEERS = sorted(
+    range(1, NY * NX), key=lambda p: -min(p // NX, NY - p // NX) - min(p % NX, NX - p % NX)
+)
 NAMES = (
     ["halo", "ow", "co0", "co1", "st0", "st1", "ret"]
     + [f"down{h}{n}" for h in range(2) for n in range(3)]
@@ -53,10 +56,7 @@
     + [f"{n}{g}" for g in range(GROUPS) for n in ("x0d", "x0r", "x1d", "x1r", "hd", "hr", "sd", "sr")]
 )
 RECV = {name: i for i, name in enumerate(NAMES)}
-SENT_NAMES = (
-    ["halo", "ow", "co", "st0", "st1", "ret", "down0", "down1", "z"]
-    + [f"{n}{g}" for g in range(GROUPS) for n in ("x0", "x1", "h", "s")]
-)
+SENT_NAMES = ("halo", "ow", "co", "st0", "st1", "ret", "down0", "down1", "z", "x", "h", "s")
 SENT = {name: i for i, name in enumerate(SENT_NAMES)}
 
 
@@ -128,18 +128,20 @@
         return (lax.rem(z + NZ - dz, NZ), lax.rem(c + NC - dc, NC), y, x)
 
     barrier = pltpu.get_barrier_semaphore()
+    loads = [
+        pltpu.make_async_copy(far, here, load_sems.at[i])
+        for i, (far, here) in enumerate(zip(away, near))
+    ]
+    for i in (1, 2, 6, 3, 0):
+        loads[i].start()
     with jax.named_scope("signals"):
-        for p in range(1, NY * NX):
+        for p in PEERS:
             py, px = in_plane(p)
             pl.semaphore_signal(barrier, inc=1, device_id=(z, c, py, px), device_id_type=MESH_ID)
         for k in range(1, NSP):
             pl.semaphore_signal(barrier, inc=1, device_id=along_z(k), device_id_type=MESH_ID)
 
-    loads = [
-        pltpu.make_async_copy(far, here, load_sems.at[i])
-        for i, (far, here) in enumerate(zip(away, near))
-    ]
-    for i in (9, 1, 2, 6, 3, 4, 0, 5, 7, 8, 10, 13, 11, 12):
+    for i in (4, 9, 5, 7, 8, 10, 13, 11, 12):
         loads[i].start()
 
     with jax.named_scope("local"):
@@ -173,7 +175,7 @@
 
     def send_mixed(part):
         cols = pl.ds(part * 128, 128)
-        for p in range(1, NY * NX):
+        for p in PEERS:
             py, px = in_plane(p)
             send(co.at[my_rows, cols], co.at[my_rows, cols], "co", f"co{part}", (z, c, py, px))
 
@@ -183,7 +185,7 @@
         co[my_rows, 128:256] = (og[:, 128:256].astype(F32) * late).astype(BF)
         send_mixed(1)
         loads[4].wait()
-        for p in range(1, NY * NX):
+        for p in PEERS:
             py, px = in_plane(p)
             there = py * NX + px
             send(
@@ -297,7 +299,7 @@
         s2 = jnp.sum(stream * stream, axis=0, keepdims=True)
         sub = lax.broadcasted_iota(jnp.int32, (2, 256), 0)
         st[which, own] = jnp.where(sub == 0, s1, s2)
-        for p in range(1, NY * NX):
+        for p in PEERS:
             py, px = in_plane(p)
             send(st.at[which, own], st.at[which, own], f"st{which}", f"st{which}", (z, c, py, px))
         if which == 0:
@@ -368,14 +370,14 @@
         for half in range(2):
             for step in steps_of(g, GATHER_DIRECT):
                 mine = slab(x4, g, half, 0, 0)
-                send(mine, mine, f"x0{g}", f"x0d{g}", ring(axis_of(half, 0), step))
+                send(mine, mine, "x", f"x0d{g}", ring(axis_of(half, 0), step))
 
     def ag_onward(g, places):
         for place in places:
             for half in range(2):
                 for step in steps_of(g, GATHER_DIRECT):
                     piece = slab(x4, g, half, 0, place)
-                    send(piece, piece, f"x1{g}", f"x1d{g}", ring(axis_of(half, 1), step))
+                    send(piece, piece, "x", f"x1d{g}", ring(axis_of(half, 1), step))
 
     def ag_relay(g, phase):
         landed(ag_like(g, phase, 2), f"x{phase}d{g}")
@@ -383,7 +385,7 @@
             for step, part in ((1, "lo"), (-1, "hi")):
                 piece = slab(x4, g, half, phase, -step, part)
                 send(
-                    piece, piece, f"x{phase}{g}", f"x{phase}r{g}", ring(axis_of(half, phase), step)
+                    piece, piece, "x", f"x{phase}r{g}", ring(axis_of(half, phase), step)
                 )
 
     def ag_end(g, phase):
@@ -412,14 +414,14 @@
         for half in range(2):
             for step in steps_of(g, SUM_DIRECT):
                 mine = hidden_at(g, half, 0)
-                send(mine, mine, f"h{g}", f"hd{g}", ring("xy"[half], step))
+                send(mine, mine, "h", f"hd{g}", ring("xy"[half], step))
 
     def hidden_relay(g):
         landed(h4.at[pl.ds(0, 2), rows_of(g), :], f"hd{g}")
         for half in range(2):
             for step, part in ((1, "lo"), (-1, "hi")):
                 piece = hidden_at(g, half, -step, part)
-                send(piece, piece, f"h{g}", f"hr{g}", ring("xy"[half], step))
+                send(piece, piece, "h", f"hr{g}", ring("xy"[half], step))
 
     def hidden_end(g):
         if g in SUM_DIRECT:
@@ -451,13 +453,13 @@
             if g in SUM_DIRECT:
                 for way, step in enumerate(steps_of(g, SUM_DIRECT)):
                     send(
-                        part_at(g, half, step), second_at(g, half, way), f"s{g}", f"sd{g}",
+                        part_at(g, half, step), second_at(g, half, way), "s", f"sd{g}",
                         ring(axis, step),
                     )
             else:
                 for way, part in ((0, "lo"), (1, "hi")):
                     send(
-                        part_at(g, half, 2, part), first_at(g, half, way), f"s{g}", f"sr{g}",
+                        part_at(g, half, 2, part), first_at(g, half, way), "s", f"sr{g}",
                         ring(axis, 1 - 2 * way),
                     )
 
@@ -470,7 +472,7 @@
                 came = first_at(g, half, way)
                 edge[...] = (edge[...].astype(F32) + came[...].astype(F32)).astype(BF)
                 send(
-                    part_at(g, half, step), second_at(g, half, way), f"s{g}", f"sd{g}",
+                    part_at(g, half, step), second_at(g, half, way), "s", f"sd{g}",
                     ring("yx"[half], step),
                 )
 
@@ -534,11 +536,9 @@
         drained(wda, "down0")
         drained(wdb, "down1")
         drained(sb.at[pl.ds(CAP, ROWS - CAP), :], "z")
-        for g in range(GROUPS):
-            drained(ag_like(g, 0, 3), f"x0{g}")
-            drained(ag_like(g, 1, 3), f"x1{g}")
-            drained(h4.at[pl.ds(0, 3), rows_of(g), :], f"h{g}")
-            drained(p4.at[pl.ds(0, 3), rows_of(g), :], f"s{g}")
+        drained(x4.at[:, :, pl.ds(0, ROWS // 16 * 15), :], "x")
+        drained(h4.at[pl.ds(0, 3)], "h")
+        drained(p4.at[pl.ds(0, 3)], "s")
     with jax.named_scope("ret_wait"):
         landed(ret.at[pl.ds(CAP, ROWS - CAP), :], "ret")
     with jax.named_scope("combine"):

time: 93 us -> 92.2 us (level)
  no operation moved by 1% of the time
where the time goes in v6:
time: 92.2 us; the launch traced here: 92.1 us
  Pallas kernels  91.4 us (99%)
    pallas_call x1, Pallas kernels, per_device(): pl.pallas_call(kernel, out_shape=jax.ShapeDtypeStruct((256, 128), BF), in...  91.4 us

profile of v6, /device:TPU:1, one launch (start us, length us, event | category | flops | bytes accessed | tf_op | source)
XLA Modules:
  0.0 92.1 jit_solution(10960434580463678581)
XLA Ops:
  0.0 91.4 %shard_map.136 = bf16[256,128]{1,0:T(8,128)(2,1)S(1)} custom-call(bf16[32,256]{1,0:T(8,128)(2,1)} %bitcast.14, bf16[32,256]{1,0:T(8,128)(2,1)} %bitcast.15, bf16[32,256]{1,0:T(8,128)(2,1)} %bitcast.16, f32[3,32]{1,0:T(4,128)} %refs_3_.1, bf16[32,2048]{1,0:T(8,128)(2,1)} %refs_4_.1, bf16[256,128]{1,0:T(8,128)(2,1)} %refs_5_.1, s32[1,256]{1,0:T(1,128)} %bitcast.19, ...), custom_call_target="tpu_custom_call" | custom-call | tf_op jit(solution)/shard_map/pallas_call | solution.py:590
  91.4 0.6 copy.16

commit v7 on v6

--- a/solution.py
+++ b/solution.py
@@ -138,7 +138,7 @@
         for p in PEERS:
             py, px = in_plane(p)
             pl.semaphore_signal(barrier, inc=1, device_id=(z, c, py, px), device_id_type=MESH_ID)
-        for k in range(1, NSP):
+        for k in range(NSP - 1, 0, -1):
             pl.semaphore_signal(barrier, inc=1, device_id=along_z(k), device_id_type=MESH_ID)
 
     for i in (4, 9, 5, 7, 8, 10, 13, 11, 12):
@@ -521,7 +521,7 @@
                 sum_second(g)
             else:
                 sum_end(g)
-                for k in ks_of(g):
+                for k in reversed(ks_of(g)):
                     cut = pl.ds(k * CAP, CAP)
                     if k == 0:
                         ret[cut, :] = ob[cut, :]

time: 92.2 us -> 91.6 us (level)
  no operation moved by 1% of the time
where the time goes in v7:
time: 91.6 us; the launch traced here: 91.5 us
  Pallas kernels  90.8 us (99%)
    pallas_call x1, Pallas kernels, per_device(): pl.pallas_call(kernel, out_shape=jax.ShapeDtypeStruct((256, 128), BF), in...  90.8 us

profile of v7, /device:TPU:1, one launch (start us, length us, event | category | flops | bytes accessed | tf_op | source)
XLA Modules:
  0.0 91.5 jit_solution(16733682565956310781)
XLA Ops:
  0.0 90.8 %shard_map.136 = bf16[256,128]{1,0:T(8,128)(2,1)S(1)} custom-call(bf16[32,256]{1,0:T(8,128)(2,1)} %bitcast.14, bf16[32,256]{1,0:T(8,128)(2,1)} %bitcast.15, bf16[32,256]{1,0:T(8,128)(2,1)} %bitcast.16, f32[3,32]{1,0:T(4,128)} %refs_3_.1, bf16[32,2048]{1,0:T(8,128)(2,1)} %refs_4_.1, bf16[256,128]{1,0:T(8,128)(2,1)} %refs_5_.1, s32[1,256]{1,0:T(1,128)} %bitcast.19, ...), custom_call_target="tpu_custom_call" | custom-call | tf_op jit(solution)/shard_map/pallas_call | solution.py:590
  90.8 0.6 copy.16
